TPU v7x, 256 devices: a whole 4x4x8 slice. The times are simulated.
256 devices in a mesh: ep: 64 (over z, x, core), tp: 4 (over y).
Axes of the slice: x: 4, y: 4, z: 8, core: 2. Of those that a mesh axis runs over, the one named last changes fastest.
Arguments:
- conv_value: bfloat16 [65536, 1024], P('ep', 'tp'), may hold values from -600 to 600
- conv_gate: bfloat16 [65536, 1024], P('ep', 'tp'), may hold values from -8 to 8
- depth_weight: float32 [31, 1024], replicated, may hold values from -1 to 1
- norm_gain: float32 [1024], replicated, may hold values from 0.1 to 1.9
- norm_shift: float32 [1024], replicated, may hold values from -3 to 3
- conv_out_weight: bfloat16 [1024, 2048], P('tp'), may hold values from -0.1875 to 0.1875
- moe_input: bfloat16 [98304, 2048], P(('ep', 'tp')), may hold values from -6 to 6
- moe_gain: float32 [2048], replicated, may hold values from 0.1 to 1.9
- route_experts: int32 [98304, 2], P(('ep', 'tp')), may hold values from 0 to 63, as said below
- route_scores: float32 [98304, 2], P(('ep', 'tp')), may hold values from -8 to 8
- expert_gate: bfloat16 [64, 2048, 512], P('ep'), may hold values from -0.125 to 0.125
- expert_up: bfloat16 [64, 2048, 512], P('ep'), may hold values from -0.125 to 0.125
- expert_down: bfloat16 [64, 512, 2048], P('ep'), may hold values from -1 to 1
Outputs:
- conv_out: bfloat16 [65536, 2048], P(('ep', 'tp'))
- moe_out: bfloat16 [98304, 2048], P(('ep', 'tp'))
Inputs may be any that keep to these rules, and one draw needn't show every extreme that they name: `route_experts`: each row names two different experts that lie in one group of 16 consecutive experts.
All inputs are finite; a program needn't handle non-finite values.
Results may differ from a plain program's by a relative error of at most 0.009.
Values may be sent and summed in bfloat16 or wider, within the bound.
A program may use at most 128 MiB of HBM per device.

v0:
```python
import jax
import jax.numpy as jnp
from jax import lax
from jax.sharding import PartitionSpec as P

CONV = 1024
TOP = 2


def passed_along(x, axis, by):
    peers = lax.axis_size(axis)
    pairs = [(i, i + by) for i in range(peers) if 0 <= i + by < peers]
    return lax.ppermute(x, axis, pairs)


def conv_half(conv_value, conv_gate, depth_weight, norm_gain, norm_shift, conv_out_weight):
    channels = conv_value.shape[1]
    length = conv_value.shape[0]
    first_col = lax.axis_index("tp") * channels
    taps = lax.dynamic_slice_in_dim(depth_weight, first_col, channels, 1)
    gains = lax.dynamic_slice_in_dim(norm_gain, first_col, channels, 0)
    shifts = lax.dynamic_slice_in_dim(norm_shift, first_col, channels, 0)
    gated = (conv_value.astype(jnp.float32) * jax.nn.sigmoid(conv_gate.astype(jnp.float32))).astype(
        jnp.bfloat16
    )
    reach = taps.shape[0] - 1
    earlier = passed_along(gated[length - reach :], "ep", 1)
    padded = jnp.concatenate([earlier, gated], 0).astype(jnp.float32)
    filtered = taps[0] * padded[0:length]
    for offset in range(1, reach + 1):
        filtered = filtered + taps[offset] * padded[offset : offset + length]
    sums, squares = lax.psum(
        (jnp.sum(filtered, axis=1), jnp.sum(filtered * filtered, axis=1)), "tp"
    )
    center = (sums / CONV)[:, None]
    spread = (squares / CONV)[:, None] - center * center
    normed = (filtered - center) * lax.rsqrt(spread + 1e-05) * gains + shifts
    activated = jax.nn.silu(normed).astype(jnp.bfloat16)
    partial_value = jnp.dot(activated, conv_out_weight, preferred_element_type=jnp.float32)
    return lax.psum_scatter(
        partial_value.astype(jnp.bfloat16).astype(jnp.float32).astype(jnp.bfloat16),
        "tp",
        scatter_dimension=0,
        tiled=True,
    )


def moe_half(moe_input, moe_gain, route_experts, route_scores, expert_gate, expert_up, expert_down):
    rows = moe_input.shape[0]
    model_width = moe_input.shape[1]
    experts_all = lax.axis_size("ep")
    capacity = 2 * (3 * TOP * rows // (4 * experts_all))
    widened = moe_input.astype(jnp.float32)
    normal_in = (
        widened * lax.rsqrt(jnp.mean(widened * widened, axis=-1, keepdims=True) + 1e-06) * moe_gain
    ).astype(jnp.bfloat16)
    chosen = route_experts.reshape(-1)
    onehot = (chosen[:, None] == jnp.arange(experts_all, dtype=jnp.int32)[None, :]).astype(
        jnp.int32
    )
    slot_rank = jnp.sum(jnp.cumsum(onehot, axis=0) * onehot, axis=-1) - 1
    slot_index = jnp.where(
        slot_rank < capacity, chosen * capacity + slot_rank, experts_all * capacity
    )
    source_row = jnp.arange(rows * TOP, dtype=jnp.int32) // TOP
    slot_token = (
        jnp.full((experts_all * capacity,), rows, jnp.int32)
        .at[slot_index]
        .set(source_row, mode="drop")
    )
    padded_in = jnp.concatenate([normal_in, jnp.zeros((1, model_width), jnp.bfloat16)], 0)
    send_buffer = padded_in[slot_token].reshape(experts_all, capacity, model_width)
    arrived = lax.all_to_all(send_buffer, "ep", split_axis=0, concat_axis=0, tiled=True)
    flat_rows = arrived.reshape(-1, model_width)
    gate_act = jnp.dot(flat_rows, expert_gate[0], preferred_element_type=jnp.float32)
    up_act = jnp.dot(flat_rows, expert_up[0], preferred_element_type=jnp.float32)
    inner = (jax.nn.silu(gate_act) * up_act).astype(jnp.bfloat16)
    result = jnp.dot(inner, expert_down[0], preferred_element_type=jnp.float32).astype(jnp.bfloat16)
    returned = lax.all_to_all(
        result.reshape(arrived.shape), "ep", split_axis=0, concat_axis=0, tiled=True
    )
    returned_flat = jnp.concatenate(
        [
            returned.reshape(experts_all * capacity, model_width),
            jnp.zeros((1, model_width), jnp.bfloat16),
        ],
        0,
    )
    picked = returned_flat[slot_index].reshape(rows, TOP, model_width)
    group_gate = jax.nn.sigmoid(route_scores[:, 0])
    first_weight = (group_gate * jax.nn.sigmoid(route_scores[:, 1]))[:, None]
    second_weight = (group_gate * jax.nn.sigmoid(-route_scores[:, 1]))[:, None]
    combined = first_weight * picked[:, 0].astype(jnp.float32) + second_weight * picked[
        :, 1
    ].astype(jnp.float32)
    return combined.astype(jnp.bfloat16)


def on_device(
    conv_value,
    conv_gate,
    depth_weight,
    norm_gain,
    norm_shift,
    conv_out_weight,
    moe_input,
    moe_gain,
    route_experts,
    route_scores,
    expert_gate,
    expert_up,
    expert_down,
):
    conv_out = conv_half(
        conv_value, conv_gate, depth_weight, norm_gain, norm_shift, conv_out_weight
    )
    moe_out = moe_half(
        moe_input, moe_gain, route_experts, route_scores, expert_gate, expert_up, expert_down
    )
    return (conv_out, moe_out)


def solution(mesh):
    in_specs = (
        P("ep", "tp"),
        P("ep", "tp"),
        P(),
        P(),
        P(),
        P("tp", None),
        P(("ep", "tp"), None),
        P(),
        P(("ep", "tp"), None),
        P(("ep", "tp"), None),
        P("ep", None, None),
        P("ep", None, None),
        P("ep", None, None),
    )
    out_specs = (P(("ep", "tp"), None), P(("ep", "tp"), None))
    return jax.shard_map(
        on_device, mesh=mesh, in_specs=in_specs, out_specs=out_specs, check_vma=False
    )
```

profile of v0, /device:TPU:2, one launch (start us, length us, event | category | flops | bytes accessed | tf_op | source)
XLA Modules:
  0.0 422.6 jit_solution(11810844819671577286)
XLA Ops:
  9.2 1.8 reduce-window.6
  11.8 3.4 scatter_custom_fusion
  15.2 1.8 fusion
  17.0 1.8 fusion.2
  20.1 12.3 %gather_fusion = bf16[1152,2048]{1,0:T(8,128)(2,1)} fusion(bf16[385,2048]{1,0:T(8,128)(2,1)} %concatenate.10, s32[2048]{0:T(1024)S(1)} %pad_clamp_fusion), kind=kCustom, calls=%fused_computation | custom fusion | bytes 9441792 | tf_op jit(solution)/shard_map/gather | solution.py:72
  32.4 7.6 %reshape.112 = bf16[64,18,2048]{2,1,0:T(8,128)(2,1)} reshape(bf16[1152,2048]{1,0:T(8,128)(2,1)} %gather_fusion) | data formatting | bytes 9437184 | tf_op jit(solution)/shard_map/reshape | solution.py:72
  40.0 12.3 %all-to-all-start = ((bf16[64,18,2048]{2,1,0:T(8,128)(2,1)}), bf16[64,18,2048]{2,1,0:T(8,128)(2,1)}, u32[]{:S(2)}, u32[]{:S(2)}) async-start(bf16[64,18,2048]{2,1,0:T(8,128)(2,1)} %reshape.112), calls=%async_computation.1 | async-start | bytes 12582912 | tf_op jit(solution)/shard_map/all_to_all | solution.py:73
  53.7 2.2 collective-permute-start
  57.2 136.3 %all-to-all-done = bf16[64,18,2048]{2,1,0:T(8,128)(2,1)} async-done(((bf16[64,18,2048]{2,1,0:T(8,128)(2,1)}), bf16[64,18,2048]{2,1,0:T(8,128)(2,1)}, u32[]{:S(2)}, u32[]{:S(2)}) %all-to-all-start) | async-done | bytes 4718624 | tf_op jit(solution)/shard_map/all_to_all | solution.py:73
  193.4 7.8 %reshape.113 = bf16[1152,2048]{1,0:T(8,128)(2,1)} reshape(bf16[64,18,2048]{2,1,0:T(8,128)(2,1)} %all-to-all-done) | data formatting | bytes 9437184 | tf_op jit(solution)/shard_map/reshape | solution.py:74
  201.2 7.1 %fusion.8 = f32[1152,512]{1,0:T(8,128)} fusion(bf16[1152,2048]{1,0:T(8,128)(2,1)} %reshape.113, bf16[1,2048,512]{2,1,0:T(8,128)(2,1)} %param.23), kind=kOutput, calls=%fused_computation.18 | convolution fusion | flops 2415919104 | bytes 9175040 | tf_op jit(solution)/shard_map/dot_general | solution.py:75
  208.3 11.0 %convolution_convert_fusion = bf16[1152,2048]{1,0:T(8,128)(2,1)} fusion(bf16[1,512,2048]{2,1,0:T(8,128)(2,1)S(1)} %copy-done, bf16[1152,2048]{1,0:T(8,128)(2,1)} %reshape.113, f32[1152,512]{1,0:T(8,128)} %fusion.8, bf16[1,2048,512]{2,1,0:T(8,128)(2,1)} %param.24), kind=kOutput, calls=%fused_computation.3 | convolution fusion | flops 4837736448 | bytes 15990784 | tf_op jit(solution)/shard_map/dot_general | solution.py:78
  219.3 7.6 %reshape.114 = bf16[64,18,2048]{2,1,0:T(8,128)(2,1)} reshape(bf16[1152,2048]{1,0:T(8,128)(2,1)} %convolution_convert_fusion) | data formatting | bytes 9437184 | tf_op jit(solution)/shard_map/reshape | solution.py:80
  226.9 5.8 %all-to-all-start.1 = ((bf16[64,18,2048]{2,1,0:T(8,128)(2,1)}), bf16[64,18,2048]{2,1,0:T(8,128)(2,1)}, u32[]{:S(2)}, u32[]{:S(2)}) async-start(bf16[64,18,2048]{2,1,0:T(8,128)(2,1)} %reshape.114), calls=%async_computation.2 | async-start | bytes 12582912 | tf_op jit(solution)/shard_map/all_to_all | solution.py:79
  235.5 4.5 %fusion.61 = (f32[1024]{0:T(1024)S(1)}, f32[1024]{0:T(1024)S(1)}, f32[1024,256]{1,0:T(8,128)S(1)}) fusion(f32[1054,256]{1,0:T(8,128)S(1)} %maximum_convert_fusion, f32[256]{0:T(256)S(1)} %bitcast.102, f32[256]{0:T(256)S(1)} %bitcast.73, f32[256]{0:T(256)S(1)} %bitcast.74, f32[256]{0:T(256)S(1)} %bitcast.75, f32[256]{0:T(256)S(1)} %bitcast.76, ...), kind=kLoop, calls=%fused_computation.130 | loop fusion | flops 16775168 | bytes 33594368 | tf_op jit(solution)/shard_map/reduce_sum | solution.py:33
  240.0 11.1 %all-reduce.2 = (f32[1024]{0:T(1024)S(1)}, f32[1024]{0:T(1024)S(1)}) all-reduce(f32[1024]{0:T(1024)S(1)} %get-tuple-element.3, f32[1024]{0:T(1024)S(1)} %get-tuple-element.2), channel_id=1, replica_groups=mesh['ep'=64,'tp'=4] {'tp'}, use_global_device_ids=true, to_apply=%region_3.0 | all-reduce | flops 2048 | bytes 16384 | tf_op jit(solution)/shard_map/psum | solution.py:32
  251.1 4.6 %convolution_convert_fusion.1 = bf16[1024,2048]{1,0:T(8,128)(2,1)} fusion(bf16[256,2048]{1,0:T(8,128)(2,1)} %param.18, f32[1024,256]{1,0:T(8,128)S(1)} %get-tuple-element.10, f32[256]{0:T(256)S(1)} %dynamic_slice.11, f32[256]{0:T(256)S(1)} %dynamic_slice.10, f32[1024]{0:T(1024)S(1)} %get-tuple-element.45, f32[1024]{0:T(1024)S(1)} %get-tuple-element.44), kind=kOutput, calls=%fused_computation.6 | convolution fusion | flops 1078198272 | bytes 6301696 | tf_op jit(solution)/shard_map/dot_general | solution.py:39
  256.4 117.4 %all-to-all-done.1 = bf16[64,18,2048]{2,1,0:T(8,128)(2,1)} async-done(((bf16[64,18,2048]{2,1,0:T(8,128)(2,1)}), bf16[64,18,2048]{2,1,0:T(8,128)(2,1)}, u32[]{:S(2)}, u32[]{:S(2)}) %all-to-all-start.1) | async-done | bytes 4718624 | tf_op jit(solution)/shard_map/all_to_all | solution.py:79
  373.9 7.8 %reshape.115 = bf16[1152,2048]{1,0:T(8,128)(2,1)} reshape(bf16[64,18,2048]{2,1,0:T(8,128)(2,1)} %all-to-all-done.1) | data formatting | bytes 9437184 | tf_op jit(solution)/shard_map/reshape | solution.py:84
  381.7 5.2 %concatenate.11 = bf16[1153,2048]{1,0:T(8,128)(2,1)} pad(bf16[1152,2048]{1,0:T(8,128)(2,1)} %reshape.115, bf16[]{:T(256)} %constant.58.clone.1), padding=0_1x0_0 | pad | bytes 9441282 | tf_op jit(solution)/shard_map/concatenate | solution.py:82
  386.8 10.0 %gather_fusion.1 = bf16[768,2048]{1,0:T(8,128)(2,1)} fusion(bf16[1153,2048]{1,0:T(8,128)(2,1)} %concatenate.11, s32[1024]{0:T(1024)S(1)} %pad_clamp_fusion.1), kind=kCustom, calls=%fused_computation.1 | custom fusion | bytes 6294528 | tf_op jit(solution)/shard_map/gather | solution.py:89
  396.9 6.0 %reshape.116 = bf16[384,2,2048]{2,1,0:T(2,128)(2,1)} reshape(bf16[768,2048]{1,0:T(8,128)(2,1)} %gather_fusion.1) | data formatting | bytes 6291456 | tf_op jit(solution)/shard_map/reshape | solution.py:89
  402.9 7.9 %fusion.63 = (bf16[384,1,2048]{2,1,0:T(2,128)(2,1)S(1)}, bf16[384,1,2048]{2,1,0:T(2,128)(2,1)S(1)}) fusion(bf16[384,2,2048]{2,1,0:T(2,128)(2,1)} %reshape.116), kind=kLoop, calls=%fused_computation.131 | loop fusion | bytes 6291456 | tf_op jit(solution)/shard_map/slice | solution.py:93
  410.9 4.9 %fusion.4 = bf16[384,2048]{1,0:T(8,128)(2,1)} fusion(bf16[384,1,2048]{2,1,0:T(2,128)(2,1)S(1)} %get-tuple-element.12, bf16[384,1,2048]{2,1,0:T(2,128)(2,1)S(1)} %get-tuple-element.11, f32[384]{0:T(512)S(1)} %get-tuple-element.5, f32[384]{0:T(512)S(1)} %get-tuple-element.4), kind=kLoop, calls=%fused_computation.13 | loop fusion | flops 4718592 | bytes 4721664 | tf_op jit(solution)/shard_map/convert_element_type | solution.py:96
  (41 shorter events, 10.1 us)
Async XLA Ops:
  7.2 201.2 %copy-start = (bf16[1,512,2048]{2,1,0:T(8,128)(2,1)S(1)}, bf16[1,512,2048]{2,1,0:T(8,128)(2,1)}, u32[]{:S(2)}) copy-start(bf16[1,512,2048]{2,1,0:T(8,128)(2,1)} %param.25) | copy-start | bytes 6291460
  7.2 9.8 %copy-start.3 = (f32[2048]{0:T(1024)S(1)}, f32[2048]{0:T(1024)}, u32[]{:S(2)}) copy-start(f32[2048]{0:T(1024)} %param.20) | copy-start | bytes 24580
  40.0 12.3 %copy-start.2 = (bf16[1024,256]{1,0:T(8,128)(2,1)S(1)}, bf16[1024,256]{1,0:T(8,128)(2,1)}, u32[]{:S(2)}) copy-start(bf16[1024,256]{1,0:T(8,128)(2,1)} %param.14) | copy-start | bytes 1572868
  40.0 153.4 %all-to-all-start = ((bf16[64,18,2048]{2,1,0:T(8,128)(2,1)}), bf16[64,18,2048]{2,1,0:T(8,128)(2,1)}, u32[]{:S(2)}, u32[]{:S(2)}) async-start(bf16[64,18,2048]{2,1,0:T(8,128)(2,1)} %reshape.112), calls=%async_computation.1 | async-start | bytes 12582912 | tf_op jit(solution)/shard_map/all_to_all | solution.py:73
  53.7 181.7 %collective-permute-start = (bf16[30,256]{1,0:T(8,128)(2,1)S(1)}, bf16[30,256]{1,0:T(8,128)(2,1)S(1)}, u32[]{:S(2)}, u32[]{:S(2)}) collective-permute-start(bf16[30,256]{1,0:T(8,128)(2,1)S(1)} %slice.281), channel_id=1, source_target_pairs={{0,4},{4,8},{8,12},{12,16},{16,20},{20,24},{24,28},{28,32},{32,36}... | collective-permute-start | bytes 46088 | tf_op jit(solution)/shard_map/ppermute | solution.py:13
  226.9 147.0 %all-to-all-start.1 = ((bf16[64,18,2048]{2,1,0:T(8,128)(2,1)}), bf16[64,18,2048]{2,1,0:T(8,128)(2,1)}, u32[]{:S(2)}, u32[]{:S(2)}) async-start(bf16[64,18,2048]{2,1,0:T(8,128)(2,1)} %reshape.114), calls=%async_computation.2 | async-start | bytes 12582912 | tf_op jit(solution)/shard_map/all_to_all | solution.py:79
  232.7 183.0 %reduce-scatter.2.cloned.1.call-start = ((), (), s32[]{:S(2)}) async-start(), calls=%async_computation.3 | async-start | bytes 5242880 | tf_op jit(solution)/shard_map/reduce_scatter | solution.py:40
  255.7 0.7 copy-start.4
  410.9 4.9 %copy-start.1 = (bf16[1,512,2048]{2,1,0:T(8,128)(2,1)S(1)}, bf16[1,512,2048]{2,1,0:T(8,128)(2,1)}, u32[]{:S(2)}) copy-start(bf16[1,512,2048]{2,1,0:T(8,128)(2,1)} %param.25) | copy-start | bytes 6291460
Sparse Core Ops, SparseCore 0:
  255.9 48.3 reduce-scatter.1
where the time goes:
time: 424 us; the launch traced here: 423 us
  waiting for transfers between devices  254 us (60%)
  local copies, waits for them, and re-layouts  83.2 us (20%)
  matrix products  22.7 us (5%)
  starting transfers between devices  20.4 us (5%)
  other arithmetic  17.3 us (4%)
  between operations  14.3 us (3%)
  blocking collectives  11.1 us (3%)
    all_to_all x1, waiting for transfers between devices, moe_half(): lax.all_to_all(send_buffer, 'ep', split_axis=0, concat_axis=0, tiled=True)  136 us
    all_to_all x1, waiting for transfers between devices, moe_half(): lax.all_to_all(result.reshape(arrived.shape), 'ep', split_axis=0, concat_...  117 us
    all_to_all x1, starting transfers between devices, moe_half(): lax.all_to_all(send_buffer, 'ep', split_axis=0, concat_axis=0, tiled=True)  12.3 us
    gather x1, local copies, waits for them, and re-layouts, moe_half(): padded_in[slot_token].reshape(experts_all, capacity, model_width)  12.3 us
    psum x1, blocking collectives, conv_half(): lax.psum((jnp.sum(filtered, axis=1), jnp.sum(filtered * filtered, axis=1)...  11.1 us
    dot_general x1, matrix products, moe_half(): jnp.dot(inner, expert_down[0], preferred_element_type=jnp.float32)  11 us
    gather x1, local copies, waits for them, and re-layouts, moe_half(): picked = returned_flat[slot_index].reshape(rows, TOP, model_width)  10 us
  transfers between devices with their start and end apart: 4, of which 2 were waited for; matrix products, arithmetic and copies ran while one was open for 21% of the time, Pallas kernels for 0%

commit v1 on v0

v1 whole, which is shorter than its diff:
```python
import functools

import jax
import jax.numpy as jnp
from jax import lax
from jax.experimental import pallas as pl
from jax.experimental.pallas import tpu as pltpu
from jax.sharding import PartitionSpec as P

CONV = 1024
TOP = 2
MESH = pl.DeviceIdType.MESH
NZ, NX, NC, NY = 8, 4, 2, 4
MAIN = 16
REM = 2
CHUNKS = 24
LAG = 10
OFFSETS = [
    (1, 0), (3, 0), (0, 1), (0, 3), (1, 1), (3, 3), (1, 3), (3, 1),
    (2, 0), (0, 2), (2, 2), (1, 2), (3, 2), (2, 1), (2, 3),
]


def passed_along(x, axis, by):
    peers = lax.axis_size(axis)
    pairs = [(i, i + by) for i in range(peers) if 0 <= i + by < peers]
    return lax.ppermute(x, axis, pairs)


def conv_half(conv_value, conv_gate, depth_weight, norm_gain, norm_shift, conv_out_weight):
    channels = conv_value.shape[1]
    length = conv_value.shape[0]
    first_col = lax.axis_index("tp") * channels
    taps = lax.dynamic_slice_in_dim(depth_weight, first_col, channels, 1)
    gains = lax.dynamic_slice_in_dim(norm_gain, first_col, channels, 0)
    shifts = lax.dynamic_slice_in_dim(norm_shift, first_col, channels, 0)
    gated = (conv_value.astype(jnp.float32) * jax.nn.sigmoid(conv_gate.astype(jnp.float32))).astype(
        jnp.bfloat16
    )
    reach = taps.shape[0] - 1
    earlier = passed_along(gated[length - reach :], "ep", 1)
    padded = jnp.concatenate([earlier, gated], 0).astype(jnp.float32)
    filtered = taps[0] * padded[0:length]
    for offset in range(1, reach + 1):
        filtered = filtered + taps[offset] * padded[offset : offset + length]
    sums, squares = lax.psum(
        (jnp.sum(filtered, axis=1), jnp.sum(filtered * filtered, axis=1)), "tp"
    )
    center = (sums / CONV)[:, None]
    spread = (squares / CONV)[:, None] - center * center
    normed = (filtered - center) * lax.rsqrt(spread + 1e-05) * gains + shifts
    activated = jax.nn.silu(normed).astype(jnp.bfloat16)
    partial_value = jnp.dot(activated, conv_out_weight, preferred_element_type=jnp.float32)
    return lax.psum_scatter(
        partial_value.astype(jnp.bfloat16).astype(jnp.float32).astype(jnp.bfloat16),
        "tp",
        scatter_dimension=0,
        tiled=True,
    )


def slot_of(expert, rank):
    high = expert // 8
    block = ((expert // 2) % 4) * NY + high % 4
    order = (expert % 2) * 2 + high // 4
    main = (block * 64 + order * MAIN).astype(jnp.float32) + rank
    rest = (1024 + block * 8 + order * REM).astype(jnp.float32) + (rank - MAIN)
    return jnp.where(rank < MAIN, main, jnp.where(rank < MAIN + REM, rest, -1.0))


def moe_kernel(
    x_hbm, gain, rt, rc, scores, wg_hbm, wu_hbm, wd_hbm, out,
    w, xn, sm, sr, rm, rr, bm, br, hg, hu, inner, rx, orx, acc,
    xsem, avail, share, foreign, ring_sent, sib_sent,
    d_sent, d_recv, r_sent, r_recv,
):
    f32, bf16 = jnp.float32, jnp.bfloat16
    ep = lax.axis_index("ep")
    y = lax.axis_index("tp")
    z, x, c = ep // 8, (ep // 2) % 4, ep % 2
    me = x * NY + y
    dd = (z - y + 8) % 4
    dist = jnp.where(c == 0, dd, (4 - dd) % 4)
    h_low = ((z - dd - y + 8) % 8) // 4
    hs = jnp.where((c == 0) | (dd == 0), h_low, 1 - h_low)

    def device(zz, xx, cc):
        return (zz * NX + xx) * NC + cc

    along = jnp.where(c == 0, (z + 1) % NZ, (z + NZ - 1) % NZ)
    ring_to = (device(along, x, c), y)
    sibling = (device(z, x, 1 - c), y)

    load_x = pltpu.make_async_copy(x_hbm, xn, xsem)
    load_x.start()

    @pl.when(dist == 0)
    def _():
        for part, ref in enumerate((wg_hbm, wu_hbm)):
            for j in range(8):
                pltpu.make_async_copy(
                    ref.at[0, pl.ds((j // 2) * 512, 512), pl.ds((j % 2) * 256, 256)],
                    w.at[hs, c, part * 8 + j],
                    avail.at[c * CHUNKS + part * 8 + j],
                ).start()
        for j in range(8):
            pltpu.make_async_copy(
                wd_hbm.at[0, :, pl.ds(j * 256, 256)],
                w.at[hs, c, 16 + j],
                avail.at[c * CHUNKS + 16 + j],
            ).start()

    barrier = pltpu.get_barrier_semaphore()
    peers = [(device(z, (x + dx) % NX, c), (y + dy) % NY) for dx, dy in OFFSETS]
    peers += [(device((z + 1) % NZ, x, c), y), (device((z + NZ - 1) % NZ, x, c), y), sibling]
    for peer in peers:
        pl.semaphore_signal(barrier, inc=1, device_id=peer, device_id_type=MESH)
    pl.semaphore_wait(barrier, len(peers))

    def ring_copy(n, sem):
        ref = w.at[hs, n // CHUNKS, n % CHUNKS]
        return pltpu.make_async_remote_copy(
            src_ref=ref, dst_ref=ref, send_sem=ring_sent, recv_sem=sem.at[n],
            device_id=ring_to, device_id_type=MESH,
        )

    def sib_copy(h, n, sem):
        ref = w.at[h, n // CHUNKS, n % CHUNKS]
        return pltpu.make_async_remote_copy(
            src_ref=ref, dst_ref=ref, send_sem=sib_sent, recv_sem=sem.at[n],
            device_id=sibling, device_id_type=MESH,
        )

    def own(n):
        ring_copy(n, avail).wait_recv()

        @pl.when(dist < 3)
        def _():
            ring_copy(n, avail).start()

        @pl.when((dist == 3) & (n % 2 == c))
        def _():
            ring_copy(n, foreign).start()

        @pl.when(dist > 0)
        def _():
            sib_copy(hs, n, share).start()

        @pl.when((dist == 0) & (n // CHUNKS == c))
        def _():
            sib_copy(hs, n, avail).start()

    def outer(n):
        @pl.when((dist == 0) & (n % 2 == c))
        def _():
            ring_copy(n, foreign).wait_recv()
            sib_copy(1 - hs, n, share).start()

    def pump(n):
        if isinstance(n, int):
            if n < 2 * CHUNKS:
                own(n)
            if n >= LAG:
                outer(n - LAG)
            return

        @pl.when(n < 2 * CHUNKS)
        def _():
            own(n)

        @pl.when(n >= LAG)
        def _():
            outer(n - LAG)

    def pumps(low, high):
        def body(n, carry):
            pump(n)
            return carry

        lax.fori_loop(low, high, body, 0)

    pump(0)

    tokens = xn.shape[0]
    first, second = rt[0:1, :], rt[1:2, :]
    ids = lax.broadcasted_iota(jnp.int32, (64, tokens), 0)
    hit0, hit1 = ids == first, ids == second
    both = jnp.where(hit0 | hit1, 1.0, 0.0).astype(bf16)
    row_t = lax.broadcasted_iota(jnp.int32, (tokens, tokens), 0)
    col_t = lax.broadcasted_iota(jnp.int32, (tokens, tokens), 1)
    earlier = jnp.where(row_t < col_t, 1.0, 0.0).astype(bf16)
    counts = jnp.dot(both, earlier, preferred_element_type=f32)
    slot0 = slot_of(first, jnp.sum(jnp.where(hit0, counts, 0.0), axis=0, keepdims=True))
    slot1 = slot_of(second, jnp.sum(jnp.where(hit1, counts, 0.0), axis=0, keepdims=True))
    first_c, second_c = rc[:, 0:1], rc[:, 1:2]
    ids_c = lax.broadcasted_iota(jnp.int32, (tokens, 64), 1)
    hit0_c, hit1_c = ids_c == first_c, ids_c == second_c
    both_c = jnp.where(hit0_c | hit1_c, 1.0, 0.0).astype(bf16)
    earlier_c = jnp.where(row_t > col_t, 1.0, 0.0).astype(bf16)
    counts_c = jnp.dot(earlier_c, both_c, preferred_element_type=f32)
    slot0_c = slot_of(first_c, jnp.sum(jnp.where(hit0_c, counts_c, 0.0), axis=1, keepdims=True))
    slot1_c = slot_of(second_c, jnp.sum(jnp.where(hit1_c, counts_c, 0.0), axis=1, keepdims=True))
    pump(1)

    load_x.wait()

    def norm(b, carry):
        rows = pl.ds(pl.multiple_of(b * 64, 64), 64)
        wide = xn[rows, :].astype(f32)
        square = jnp.mean(wide * wide, axis=-1, keepdims=True)
        xn[rows, :] = (wide * lax.rsqrt(square + 1e-06) * gain[...]).astype(bf16)
        return carry

    for part in range(3):
        lax.fori_loop(part * 2, part * 2 + 2, norm, 0)
        pump(2 + part)

    def picked(base, count):
        at = (lax.broadcasted_iota(jnp.int32, (count, tokens), 0) + base).astype(f32)
        return jnp.where((at == slot0) | (at == slot1), 1.0, 0.0).astype(bf16)

    def gather(g, carry):
        choose = picked(g * 256, 256)

        def cols(q, carry):
            at = pl.ds(pl.multiple_of(q * 512, 512), 512)
            rows = jnp.dot(choose, xn[:, at], preferred_element_type=f32).astype(bf16)
            sm[pl.ds(g * 4, 4), :, at] = rows.reshape(4, 64, 512)
            return carry

        lax.fori_loop(0, 4, cols, 0)
        pump(5 + g)
        return carry

    lax.fori_loop(0, 4, gather, 0)
    choose = picked(1024, 128)

    def gather_rest(q, carry):
        at = pl.ds(pl.multiple_of(q * 512, 512), 512)
        rows = jnp.dot(choose, xn[:, at], preferred_element_type=f32)
        sr[:, :, at] = rows.reshape(16, 8, 512).astype(bf16)
        return carry

    lax.fori_loop(0, 4, gather_rest, 0)

    def block_at(k, sign):
        dx, dy = OFFSETS[k]
        xx, yy = (x + sign * dx + NX) % NX, (y + sign * dy + NY) % NY
        return xx * NY + yy, (device(z, xx, c), yy)

    def dispatch(k, part):
        block, peer = block_at(k, 1)
        if part < 2:
            src, dst = sm.at[block, pl.ds(part * 32, 32)], rm.at[me, pl.ds(part * 32, 32)]
        else:
            src, dst = sr.at[block], rr.at[me]
        return pltpu.make_async_remote_copy(
            src_ref=src, dst_ref=dst, send_sem=d_sent.at[part, k], recv_sem=d_recv.at[part, k],
            device_id=peer, device_id_type=MESH,
        )

    for part in range(3):
        for k in range(15):
            dispatch(k, part).start()
    rm[me] = sm[me]
    rr[me] = sr[me]

    pumps(9, 24)

    for part in range(3):
        for k in range(15):
            dispatch(k, part).wait_recv()
    rx[...] = rr[...].astype(f32).reshape(128, 2048).astype(bf16)
    hg[...] = jnp.zeros_like(hg)
    hu[...] = jnp.zeros_like(hu)

    def rows_of(cc, h, at):
        main = rm[:, cc * 32 + h * MAIN : cc * 32 + (h + 1) * MAIN, at]
        return jnp.concatenate([main.reshape(256, main.shape[2]), rx[:, at]], axis=0)

    order_in_rest = (lax.broadcasted_iota(jnp.int32, (128, 256), 0) % 8) // REM

    def ffn(cc, j):
        n = cc * CHUNKS + j

        @pl.when((dist > 0) | (n % 2 != c))
        def _():
            sib_copy(hs, n, share).wait_recv()

        at_k = pl.ds(pl.multiple_of(((j % 8) // 2) * 512, 512), 512)
        at_n = pl.ds(pl.multiple_of((j % 2) * 256, 256), 256)
        at_o = pl.ds(pl.multiple_of((j % 8) * 256, 256), 256)
        for h in range(2):

            @pl.when(j < 8)
            def _(h=h):
                hg[h, :, at_n] += jnp.dot(
                    rows_of(cc, h, at_k), w[h, cc, j], preferred_element_type=f32
                )

            @pl.when((j >= 8) & (j < 16))
            def _(h=h):
                hu[h, :, at_n] += jnp.dot(
                    rows_of(cc, h, at_k), w[h, cc, j], preferred_element_type=f32
                )

            @pl.when(j == 15)
            def _(h=h):
                gate = hg[h]
                inner[h] = (jax.nn.silu(gate) * hu[h]).astype(bf16)
                hg[h] = jnp.zeros_like(gate)
                hu[h] = jnp.zeros_like(gate)

            @pl.when(j >= 16)
            def _(h=h):
                rows = jnp.dot(inner[h], w[h, cc, j], preferred_element_type=f32)
                rm[:, cc * 32 + h * MAIN : cc * 32 + (h + 1) * MAIN, at_o] = (
                    rows[:256].astype(bf16).reshape(16, MAIN, 256)
                )
                mine = order_in_rest == cc * 2 + h
                orx[:, at_o] = jnp.where(mine, rows[256:], orx[:, at_o])

    def phase0(n, carry):
        pump(n)
        ffn(0, 2 * (n - 24))
        ffn(0, 2 * (n - 24) + 1)
        return carry

    lax.fori_loop(24, 36, phase0, 0)

    def back(k, part):
        block, peer = block_at(k, -1)
        if part < 2:
            src, dst = rm.at[block, pl.ds(part * 32, 32)], bm.at[me, pl.ds(part * 32, 32)]
        else:
            src, dst = rr.at[block], br.at[me]
        return pltpu.make_async_remote_copy(
            src_ref=src, dst_ref=dst, send_sem=r_sent.at[part, k], recv_sem=r_recv.at[part, k],
            device_id=peer, device_id_type=MESH,
        )

    for k in range(15):
        back(k, 0).start()
    bm[me, 0:32] = rm[me, 0:32]

    def phase1(n, carry):
        pump(n)
        j = n - LAG - CHUNKS

        @pl.when(n < 38)
        def _():
            ffn(1, 2 * (n - 36))
            ffn(1, 2 * (n - 36) + 1)

        @pl.when(n >= 38)
        def _():
            ffn(1, j)

        return carry

    lax.fori_loop(36, 2 * CHUNKS + LAG, phase1, 0)

    rr[...] = orx[...].reshape(16, 8, 2048).astype(bf16)
    for part in (1, 2):
        for k in range(15):
            back(k, part).start()
    bm[me, 32:64] = rm[me, 32:64]
    br[me] = rr[me]

    group = jax.nn.sigmoid(scores[:, 0:1])
    weight0 = group * jax.nn.sigmoid(scores[:, 1:2])
    weight1 = group * jax.nn.sigmoid(-scores[:, 1:2])

    def chosen(slot, cc):
        at = lax.broadcasted_iota(jnp.int32, (tokens, 512), 1)
        main = ((at // 32) * 64 + cc * 32 + at % 32).astype(f32)
        hits = jnp.where(main == slot, 1.0, 0.0).astype(bf16)
        if cc == 0:
            return hits
        rest = (lax.broadcasted_iota(jnp.int32, (tokens, 128), 1) + 1024).astype(f32)
        return jnp.concatenate([hits, jnp.where(rest == slot, 1.0, 0.0).astype(bf16)], axis=1)

    for k in range(15):
        back(k, 0).wait_recv()
    pick0, pick1 = chosen(slot0_c, 0), chosen(slot1_c, 0)

    def combine0(q, carry):
        at = pl.ds(pl.multiple_of(q * 512, 512), 512)
        rows = bm[:, 0:32, at].reshape(512, 512)
        acc[:, at] = weight0 * jnp.dot(
            pick0, rows, preferred_element_type=f32
        ) + weight1 * jnp.dot(pick1, rows, preferred_element_type=f32)
        return carry

    lax.fori_loop(0, 4, combine0, 0)

    for part in (1, 2):
        for k in range(15):
            back(k, part).wait_recv()
    pick0b, pick1b = chosen(slot0_c, 1), chosen(slot1_c, 1)

    def combine1(q, carry):
        at = pl.ds(pl.multiple_of(q * 512, 512), 512)
        rest = br[:, :, at].astype(f32).reshape(128, 512).astype(bf16)
        rows = jnp.concatenate([bm[:, 32:64, at].reshape(512, 512), rest], axis=0)
        total = acc[:, at] + (
            weight0 * jnp.dot(pick0b, rows, preferred_element_type=f32)
            + weight1 * jnp.dot(pick1b, rows, preferred_element_type=f32)
        )
        out[:, at] = total.astype(bf16)
        return carry

    lax.fori_loop(0, 4, combine1, 0)

    for part in range(3):
        for k in range(15):
            dispatch(k, part).wait_send()
            back(k, part).wait_send()

    def sent(n, carry):
        @pl.when((dist < 3) | (n % 2 == c))
        def _():
            ring_copy(n, avail).wait_send()

        sib_copy(hs, n, share).wait_send()
        return carry

    lax.fori_loop(0, 2 * CHUNKS, sent, 0)


def moe_half(moe_input, moe_gain, route_experts, route_scores, expert_gate, expert_up, expert_down):
    bf16, f32 = jnp.bfloat16, jnp.float32
    rows, width = moe_input.shape
    hbm = pl.BlockSpec(memory_space=pl.ANY)
    vmem = pl.BlockSpec(memory_space=pltpu.VMEM)
    dma = pltpu.SemaphoreType.DMA
    return pl.pallas_call(
        moe_kernel,
        out_shape=jax.ShapeDtypeStruct((rows, width), bf16),
        in_specs=[hbm, vmem, vmem, vmem, vmem, hbm, hbm, hbm],
        out_specs=vmem,
        scratch_shapes=[
            pltpu.VMEM((2, 2, CHUNKS, 512, 256), bf16),
            pltpu.VMEM((rows, width), bf16),
            pltpu.VMEM((16, 64, width), bf16),
            pltpu.VMEM((16, 8, width), bf16),
            pltpu.VMEM((16, 64, width), bf16),
            pltpu.VMEM((16, 8, width), bf16),
            pltpu.VMEM((16, 64, width), bf16),
            pltpu.VMEM((16, 8, width), bf16),
            pltpu.VMEM((2, 384, 512), f32),
            pltpu.VMEM((2, 384, 512), f32),
            pltpu.VMEM((2, 384, 512), bf16),
            pltpu.VMEM((128, width), bf16),
            pltpu.VMEM((128, width), f32),
            pltpu.VMEM((rows, width), f32),
            dma,
            dma((2 * CHUNKS,)),
            dma((2 * CHUNKS,)),
            dma((2 * CHUNKS,)),
            dma,
            dma,
            dma((3, 15)),
            dma((3, 15)),
            dma((3, 15)),
            dma((3, 15)),
        ],
        compiler_params=pltpu.CompilerParams(
            collective_id=0, has_side_effects=True, vmem_limit_bytes=66_000_000
        ),
        name="experts",
    )(
        moe_input,
        moe_gain.reshape(1, width),
        route_experts.T,
        route_experts,
        route_scores,
        expert_gate,
        expert_up,
        expert_down,
    )


def on_device(
    conv_value,
    conv_gate,
    depth_weight,
    norm_gain,
    norm_shift,
    conv_out_weight,
    moe_input,
    moe_gain,
    route_experts,
    route_scores,
    expert_gate,
    expert_up,
    expert_down,
):
    conv_out = conv_half(
        conv_value, conv_gate, depth_weight, norm_gain, norm_shift, conv_out_weight
    )
    moe_out = moe_half(
        moe_input, moe_gain, route_experts, route_scores, expert_gate, expert_up, expert_down
    )
    return (conv_out, moe_out)


def solution(mesh):
    in_specs = (
        P("ep", "tp"),
        P("ep", "tp"),
        P(),
        P(),
        P(),
        P("tp", None),
        P(("ep", "tp"), None),
        P(),
        P(("ep", "tp"), None),
        P(("ep", "tp"), None),
        P("ep", None, None),
        P("ep", None, None),
        P("ep", None, None),
    )
    out_specs = (P(("ep", "tp"), None), P(("ep", "tp"), None))
    return jax.shard_map(
        on_device, mesh=mesh, in_specs=in_specs, out_specs=out_specs, check_vma=False
    )
```

time: 424 us -> 281 us (0.66)
  waiting for transfers between devices: 254 us -> 0.04 us
  Pallas kernels: 0 us -> 234 us
  local copies, waits for them, and re-layouts: 83.2 us -> 8.87 us
  matrix products: 22.7 us -> 3.37 us
  starting transfers between devices: 20.4 us -> 1.96 us
  other arithmetic: 17.3 us -> 6.14 us
    all_to_all x2 -> x0, waiting for transfers between devices: 254 us -> none  [the longest x1 136 us: moe_half(): lax.all_to_all(send_buffer, 'ep', split_axis=0, concat_axis=0, tiled=True)]
    pallas_call x0 -> x1, Pallas kernels: none -> 234 us  [moe_half(): pl.pallas_call(moe_kernel, out_shape=jax.ShapeDtypeStruct((rows, width),...]
    reshape x5 -> x0, local copies, waits for them, and re-layouts: 36.7 us -> none  [the longest x1 7.77 us: moe_half(): flat_rows = arrived.reshape(-1, model_width)]
    gather x2 -> x0, local copies, waits for them, and re-layouts: 22.3 us -> none  [the longest x1 12.3 us: moe_half(): padded_in[slot_token].reshape(experts_all, capacity, model_width)]
    dot_general x2 -> x0, matrix products: 18.1 us -> none  [the longest x1 11 us: moe_half(): jnp.dot(inner, expert_down[0], preferred_element_type=jnp.float32)]
    all_to_all x2 -> x0, starting transfers between devices: 18.1 us -> none  [the longest x1 12.3 us: moe_half(): lax.all_to_all(send_buffer, 'ep', split_axis=0, concat_axis=0, tiled=True)]
    slice x2 -> x0, local copies, waits for them, and re-layouts: 8.21 us -> none  [the longest x1 7.93 us: moe_half(): picked[:, 0].astype(jnp.float32)]
    convert_element_type x3 -> x0, other arithmetic: 6.73 us -> none  [the longest x1 4.88 us: moe_half(): return combined.astype(jnp.bfloat16)]
  transfers between devices with their start and end apart: 4 -> 2, of which waited for: 2 -> 0; matrix products, arithmetic and copies ran while one was open for 21% -> 2% of each run, Pallas kernels for 0% -> 84%
where the time goes in v1:
time: 281 us; the launch traced here: 279 us
  Pallas kernels  234 us (83%)
  between operations  14.1 us (5%)
  blocking collectives  10.9 us (4%)
  local copies, waits for them, and re-layouts  8.87 us (3%)
  other arithmetic  6.14 us (2%)
  matrix products  3.37 us (1%)
    pallas_call x1, Pallas kernels, moe_half(): pl.pallas_call(moe_kernel, out_shape=jax.ShapeDtypeStruct((rows, width),...  234 us
    psum x1, blocking collectives, conv_half(): lax.psum((jnp.sum(filtered, axis=1), jnp.sum(filtered * filtered, axis=1)...  10.9 us
  transfers between devices with their start and end apart: 2, of which 0 were waited for; matrix products, arithmetic and copies ran while one was open for 2% of the time, Pallas kernels for 84%

profile of v1, /device:TPU:2, one launch (start us, length us, event | category | flops | bytes accessed | tf_op | source)
XLA Modules:
  0.0 279.0 jit_solution(8257826558059800706)
XLA Ops:
  7.2 0.0 reduce-scatter.2.cloned.1.call-start
  7.2 1.5 multiply_convert_fusion.1
  8.7 1.9 collective-permute-start
  10.7 1.2 constant_dynamic-slice_fusion
  11.9 1.1 fusion.38
  13.0 0.8 dynamic_slice.10
  13.7 0.8 dynamic_slice.11
  14.5 0.0 collective-permute-done
  14.5 0.1 maximum_convert_fusion
  14.6 0.0 copy-start.2
  14.6 4.5 %fusion.36 = (f32[1024]{0:T(1024)S(1)}, f32[1024]{0:T(1024)S(1)}, f32[1024,256]{1,0:T(8,128)S(1)}) fusion(f32[1054,256]{1,0:T(8,128)S(1)} %maximum_convert_fusion, f32[256]{0:T(256)S(1)} %bitcast.66, f32[256]{0:T(256)S(1)} %bitcast.37, f32[256]{0:T(256)S(1)} %bitcast.38, f32[256]{0:T(256)S(1)} %bitcast.39, f32[256]{0:T(256)S(1)} %bitcast.40, ...), kind=kLoop, calls=%fused_computation.75 | loop fusion | flops 16775168 | bytes 33594368 | tf_op jit(solution)/shard_map/reduce_sum | solution.py:47
  19.1 10.9 %all-reduce = (f32[1024]{0:T(1024)S(1)}, f32[1024]{0:T(1024)S(1)}) all-reduce(f32[1024]{0:T(1024)S(1)} %get-tuple-element.3, f32[1024]{0:T(1024)S(1)} %get-tuple-element.2), channel_id=1, replica_groups=mesh['ep'=64,'tp'=4] {'tp'}, use_global_device_ids=true, to_apply=%region_3.0 | all-reduce | flops 2048 | bytes 16384 | tf_op jit(solution)/shard_map/psum | solution.py:46
  30.1 0.0 copy-done.2
  30.1 3.4 %convolution_convert_fusion = bf16[1024,2048]{1,0:T(8,128)(2,1)} fusion(bf16[256,2048]{1,0:T(8,128)(2,1)S(1)} %copy-done.2, f32[1024,256]{1,0:T(8,128)S(1)} %get-tuple-element.6, f32[256]{0:T(256)S(1)} %dynamic_slice.11, f32[256]{0:T(256)S(1)} %dynamic_slice.10, f32[1024]{0:T(1024)S(1)} %get-tuple-element.39, f32[1024]{0:T(1024)S(1)} %get-tuple-element.38), kind=kOutput, calls=%fused_computation | convolution fusion | flops 1078198272 | bytes 6301696 | tf_op jit(solution)/shard_map/dot_general | solution.py:53
  33.4 0.0 copy-start
  33.4 0.0 copy-start.1
  33.4 0.0 reduce-scatter.2.cloned.1.call-update
  33.5 0.7 copy-done
  34.1 0.8 copy.15.rc
  35.0 0.0 copy-done.1
  35.0 0.8 copy.16.scores
  35.8 233.6 %experts.1 = bf16[384,2048]{1,0:T(8,128)(2,1)} custom-call(bf16[384,2048]{1,0:T(8,128)(2,1)} %x_hbm.1, f32[1,2048]{1,0:T(1,128)} %bitcast.35, s32[2,384]{1,0:T(2,128)} %bitcast.34, s32[384,2]{1,0:T(8,128)} %copy.15.rc, f32[384,2]{1,0:T(8,128)} %copy.16.scores, bf16[1,2048,512]{2,1,0:T(8,128)(2,1)} %wg_hbm.1, bf16[1,2048,512]{2,1,0:T(8,128)(2,1)} %wu_hbm.1, ...), custom_call_target="tpu_custom_call" | custom-call | tf_op jit(solution)/shard_map/experts/pallas_call | solution.py:437
  269.4 0.0 reduce-scatter.2.cloned.1.call-done
  269.5 2.7 copy.18
  (2 shorter events, 0.0 us)
Async XLA Ops:
  7.2 262.3 %reduce-scatter.2.cloned.1.call-start = ((), (), s32[]{:S(2)}) async-start(), calls=%async_computation.1 | async-start | bytes 5242880 | tf_op jit(solution)/shard_map/reduce_scatter | solution.py:54
  8.7 5.7 %collective-permute-start = (bf16[30,256]{1,0:T(8,128)(2,1)S(1)}, bf16[30,256]{1,0:T(8,128)(2,1)S(1)}, u32[]{:S(2)}, u32[]{:S(2)}) collective-permute-start(bf16[30,256]{1,0:T(8,128)(2,1)S(1)} %slice.252), channel_id=1, source_target_pairs={{0,4},{4,8},{8,12},{12,16},{16,20},{20,24},{24,28},{28,32},{32,36}... | collective-permute-start | bytes 46088 | tf_op jit(solution)/shard_map/ppermute | solution.py:27
  14.6 15.5 %copy-start.2 = (bf16[256,2048]{1,0:T(8,128)(2,1)S(1)}, bf16[256,2048]{1,0:T(8,128)(2,1)}, u32[]{:S(2)}) copy-start(bf16[256,2048]{1,0:T(8,128)(2,1)} %param.18) | copy-start | bytes 3145732
  33.4 0.7 copy-start
  33.4 1.5 copy-start.1
Sparse Core Ops, SparseCore 0:
  33.6 107.2 reduce-scatter.1

commit v2 on v0

v2 whole, which is shorter than its diff:
```python
import jax
import jax.numpy as jnp
from jax import lax
from jax.experimental import pallas as pl
from jax.experimental.pallas import tpu as pltpu
from jax.sharding import PartitionSpec as P

MESH = pl.DeviceIdType.MESH
NZ, NX, NC, NY = 8, 4, 2, 4
CONV = 1024
KERNEL = 31
HALO = 32
MAIN = 16
REM = 2
CHUNKS = 24
TOTAL = 2 * CHUNKS
HOP = 2
FAR = 4 * HOP + 1
START = 28
OFFSETS = [
    (1, 0), (3, 0), (0, 1), (0, 3), (1, 1), (3, 3), (1, 3), (3, 1),
    (2, 0), (0, 2), (2, 2), (1, 2), (3, 2), (2, 1), (2, 3),
]


def slot_of(expert, rank):
    high = expert // 8
    block = ((expert // 2) % 4) * NY + high % 4
    order = (expert % 2) * 2 + high // 4
    main = (block * 64 + order * MAIN).astype(jnp.float32) + rank
    rest = (1024 + block * 8 + order * REM).astype(jnp.float32) + (rank - MAIN)
    return jnp.where(rank < MAIN, main, jnp.where(rank < MAIN + REM, rest, -1.0))


def eye(n):
    return lax.broadcasted_iota(jnp.int32, (n, n), 0) == lax.broadcasted_iota(jnp.int32, (n, n), 1)


def to_column(row, n):
    pieces = []
    for at in range(0, n, 128):
        spread = jnp.where(eye(128), row[:, at : at + 128], 0.0)
        pieces.append(jnp.sum(spread, axis=1, keepdims=True))
    return pieces[0] if len(pieces) == 1 else jnp.concatenate(pieces, axis=0)


def to_row(column):
    return jnp.sum(jnp.where(eye(128), column, 0.0), axis=0, keepdims=True)


def kernel(
    value_hbm, gate_hbm, taps_hbm, gain_c, shift_c, cw_hbm,
    x_hbm, gain, table, wg_hbm, wu_hbm, wd_hbm,
    conv_out, out,
    w, xn, sm, sr, rm, rr, bm, br, hg, hu, inner, rx, orx, acc,
    val, gat, taps, pad, filt, act, acts, cw, window, halo_out, halo_in, stat, stats,
    load, avail, share, foreign, ring_sent, sib_sent,
    d_sent, d_recv, r_sent, r_recv, q_sent, q_recv,
    halo_sem, stat_sent, stat_recv, act_sent, act_recv, cw_sent, cw_recv, cs_sent, cs_recv,
):
    f32, bf16 = jnp.float32, jnp.bfloat16
    ep = lax.axis_index("ep")
    y = lax.axis_index("tp")
    z, x, c = ep // 8, (ep // 2) % 4, ep % 2
    me = x * NY + y
    dd = (z - y + 8) % 4
    dist = jnp.where(c == 0, dd, (4 - dd) % 4)
    h_low = ((z - dd - y + 8) % 8) // 4
    hs = jnp.where((c == 0) | (dd == 0), h_low, 1 - h_low)

    def device(zz, xx, cc):
        return (zz * NX + xx) * NC + cc

    along = jnp.where(c == 0, (z + 1) % NZ, (z + NZ - 1) % NZ)
    ring_to = (device(along, x, c), y)
    sibling = (device(z, x, 1 - c), y)
    my_cols = pl.ds(pl.multiple_of(y * 256, 256), 256)

    loads = [
        pltpu.make_async_copy(value_hbm, val, load.at[0]),
        pltpu.make_async_copy(gate_hbm, gat, load.at[1]),
        pltpu.make_async_copy(x_hbm, xn, load.at[2]),
        pltpu.make_async_copy(taps_hbm.at[:, my_cols], taps, load.at[3]),
        pltpu.make_async_copy(cw_hbm, cw.at[y], load.at[4]),
    ]

    @pl.when(dist == 0)
    def _():
        for part, ref in enumerate((wg_hbm, wu_hbm)):
            for j in range(8):
                pltpu.make_async_copy(
                    ref.at[0, pl.ds((j // 2) * 512, 512), pl.ds((j % 2) * 256, 256)],
                    w.at[hs, c, part * 8 + j],
                    avail.at[c * CHUNKS + part * 8 + j],
                ).start()
        for j in range(8):
            pltpu.make_async_copy(
                wd_hbm.at[0, :, pl.ds(j * 256, 256)],
                w.at[hs, c, 16 + j],
                avail.at[c * CHUNKS + 16 + j],
            ).start()

    for copy in loads:
        copy.start()

    with jax.named_scope("s_barrier"):
        barrier = pltpu.get_barrier_semaphore()
        peers = [(device(z, (x + dx) % NX, c), (y + dy) % NY) for dx, dy in OFFSETS]
        peers += [(device((z + 1) % NZ, x, c), y), (device((z + NZ - 1) % NZ, x, c), y), sibling]
        peers += [((ep + 1) % 64, y), ((ep + 63) % 64, y)]
        for peer in peers:
            pl.semaphore_signal(barrier, inc=1, device_id=peer, device_id_type=MESH)
        pl.semaphore_wait(barrier, len(peers))

    def ring_copy(n, sem):
        ref = w.at[hs, n // CHUNKS, n % CHUNKS]
        return pltpu.make_async_remote_copy(
            src_ref=ref, dst_ref=ref, send_sem=ring_sent, recv_sem=sem.at[n],
            device_id=ring_to, device_id_type=MESH,
        )

    def sib_copy(h, n, sem):
        ref = w.at[h, n // CHUNKS, n % CHUNKS]
        return pltpu.make_async_remote_copy(
            src_ref=ref, dst_ref=ref, send_sem=sib_sent, recv_sem=sem.at[n],
            device_id=sibling, device_id_type=MESH,
        )

    def own(n):
        ring_copy(n, avail).wait_recv()

        @pl.when(dist < 3)
        def _():
            ring_copy(n, avail).start()

        @pl.when((dist == 3) & (n % 2 == c))
        def _():
            ring_copy(n, foreign).start()

        @pl.when(dist > 0)
        def _():
            sib_copy(hs, n, share).start()

        @pl.when((dist == 0) & (n // CHUNKS == c))
        def _():
            sib_copy(hs, n, avail).start()

    def step(p):
        n = p - HOP * dist
        m = p - FAR

        @pl.when((n >= 0) & (n < TOTAL))
        def _():
            own(n)

        @pl.when((dist == 0) & (m >= 0) & (m < TOTAL) & (m % 2 == c))
        def _():
            ring_copy(m, foreign).wait_recv()
            sib_copy(1 - hs, m, share).start()

    step(0)

    with jax.named_scope("s_gated"):
        loads[0].wait()
        loads[1].wait()

        def gated(b, carry):
            rows = pl.ds(pl.multiple_of(b * 128, 128), 128)
            wide = val[rows, :].astype(f32) * jax.nn.sigmoid(gat[rows, :].astype(f32))
            pad[pl.ds(pl.multiple_of(HALO + b * 128, 32), 128), :] = wide.astype(bf16).astype(f32)
            return carry

        lax.fori_loop(0, 8, gated, 0)
        halo_out[...] = pad[1024 : 1024 + HALO, :].astype(bf16)
        halo = pltpu.make_async_remote_copy(
            src_ref=halo_out, dst_ref=halo_in, send_sem=halo_sem.at[0], recv_sem=halo_sem.at[1],
            device_id=((ep + 1) % 64, y), device_id_type=MESH,
        )
        halo.start()

    step(1)

    with jax.named_scope("s_route"):
        tokens = xn.shape[0]
        first, second = table[0:1, :].astype(jnp.int32), table[1:2, :].astype(jnp.int32)
        ids = lax.broadcasted_iota(jnp.int32, (64, tokens), 0)
        hit0, hit1 = ids == first, ids == second
        both = jnp.where(hit0 | hit1, 1.0, 0.0).astype(bf16)
        row_t = lax.broadcasted_iota(jnp.int32, (tokens, tokens), 0)
        col_t = lax.broadcasted_iota(jnp.int32, (tokens, tokens), 1)
        earlier = jnp.where(row_t < col_t, 1.0, 0.0).astype(bf16)
        counts = jnp.dot(both, earlier, preferred_element_type=f32)
        slot0 = slot_of(first, jnp.sum(jnp.where(hit0, counts, 0.0), axis=0, keepdims=True))
        slot1 = slot_of(second, jnp.sum(jnp.where(hit1, counts, 0.0), axis=0, keepdims=True))

    with jax.named_scope("s_norm"):
        loads[2].wait()

        def norm(b, carry):
            rows = pl.ds(pl.multiple_of(b * 64, 64), 64)
            wide = xn[rows, :].astype(f32)
            square = jnp.mean(wide * wide, axis=-1, keepdims=True)
            xn[rows, :] = (wide * lax.rsqrt(square + 1e-06) * gain[...]).astype(bf16)
            return carry

        lax.fori_loop(0, 6, norm, 0)
    step(2)

    def picked(base, count):
        at = (lax.broadcasted_iota(jnp.int32, (count, tokens), 0) + base).astype(f32)
        return jnp.where((at == slot0) | (at == slot1), 1.0, 0.0).astype(bf16)

    def gather(g, carry):
        choose = picked(g * 256, 256)

        def cols(q, carry):
            at = pl.ds(pl.multiple_of(q * 512, 512), 512)
            rows = jnp.dot(choose, xn[:, at], preferred_element_type=f32).astype(bf16)
            sm[pl.ds(g * 4, 4), :, at] = rows.reshape(4, 64, 512)
            return carry

        lax.fori_loop(0, 4, cols, 0)

        @pl.when(g % 2 == 1)
        def _():
            step(3 + g // 2)

        return carry

    with jax.named_scope("s_gather"):
        lax.fori_loop(0, 4, gather, 0)
        choose = picked(1024, 128)

        def gather_rest(q, carry):
            at = pl.ds(pl.multiple_of(q * 512, 512), 512)
            rows = jnp.dot(choose, xn[:, at], preferred_element_type=f32)
            sr[:, :, at] = rows.reshape(16, 8, 512).astype(bf16)
            return carry

        lax.fori_loop(0, 4, gather_rest, 0)

    def block_at(k, sign):
        dx, dy = OFFSETS[k]
        xx, yy = (x + sign * dx + NX) % NX, (y + sign * dy + NY) % NY
        return xx * NY + yy, (device(z, xx, c), yy)

    def dispatch(k, part):
        block, peer = block_at(k, 1)
        if part < 2:
            src, dst = sm.at[block, pl.ds(part * 32, 32)], rm.at[me, pl.ds(part * 32, 32)]
        else:
            src, dst = sr.at[block], rr.at[me]
        return pltpu.make_async_remote_copy(
            src_ref=src, dst_ref=dst, send_sem=d_sent.at[part, k], recv_sem=d_recv.at[part, k],
            device_id=peer, device_id_type=MESH,
        )

    with jax.named_scope("s_dispatch"):
        for part in range(3):
            for k in range(15):
                dispatch(k, part).start()
        rm[me] = sm[me]
        rr[me] = sr[me]

    with jax.named_scope("s_filter"):
        halo.wait_recv()
        pad[0:HALO, :] = jnp.where(ep > 0, halo_in[...].astype(f32), 0.0)
        loads[3].wait()

        def filter_block(b, carry):
            step(5 + b)
            base = pl.multiple_of(b * 128, 128)
            window[...] = pad[pl.ds(base, 128 + HALO), :]
            total = None
            for k in range(KERNEL):
                low = HALO - KERNEL + 1 + k
                term = taps[k : k + 1, :] * window[low : low + 128, :]
                total = term if total is None else total + term
            filt[pl.ds(base, 128), :] = total
            stat[y, pl.ds(b, 1), :] = to_row(jnp.sum(total, axis=1, keepdims=True))
            stat[y, pl.ds(8 + b, 1), :] = to_row(jnp.sum(total * total, axis=1, keepdims=True))
            return carry

        lax.fori_loop(0, 8, filter_block, 0)

    def near(k):
        yy = (y + k) % NY
        return yy, (ep, yy)

    def stat_copy(k):
        return pltpu.make_async_remote_copy(
            src_ref=stat.at[y], dst_ref=stat.at[y], send_sem=stat_sent.at[k], recv_sem=stat_recv.at[k],
            device_id=near(k)[1], device_id_type=MESH,
        )

    def act_copy(k):
        yy, peer = near(k)
        return pltpu.make_async_remote_copy(
            src_ref=act.at[pl.ds(pl.multiple_of(yy * 256, 256), 256)], dst_ref=acts.at[y],
            send_sem=act_sent.at[k], recv_sem=act_recv.at[k], device_id=peer, device_id_type=MESH,
        )

    half = pl.ds(pl.multiple_of(c * 128, 128), 128)

    def cw_copy(k):
        return pltpu.make_async_remote_copy(
            src_ref=cw.at[y, half], dst_ref=cw.at[y, half], send_sem=cw_sent.at[k],
            recv_sem=cw_recv.at[k], device_id=near(k)[1], device_id_type=MESH,
        )

    def cs_copy(k):
        yy = (y + NY - k) % NY
        return pltpu.make_async_remote_copy(
            src_ref=cw.at[yy, half], dst_ref=cw.at[yy, half], send_sem=cs_sent.at[k],
            recv_sem=cs_recv.at[k], device_id=sibling, device_id_type=MESH,
        )

    loads[4].wait()
    for k in (1, 3, 2):
        stat_copy(k).start()
    for k in (1, 3, 2):
        cw_copy(k).start()

    def only_step(p, carry):
        step(p)
        return carry

    with jax.named_scope("s_pumps"):
        lax.fori_loop(13, START, only_step, 0)

    with jax.named_scope("s_wait_rows"):
        for part in range(3):
            for k in range(15):
                dispatch(k, part).wait_recv()
        rx[...] = rr[...].astype(f32).reshape(128, 2048).astype(bf16)
        hg[...] = jnp.zeros_like(hg)
        hu[...] = jnp.zeros_like(hu)

    with jax.named_scope("s_wait_stat"):
        for k in (1, 3, 2):
            stat_copy(k).wait_recv()
        stats[...] = (stat[0] + stat[1]) + (stat[2] + stat[3])

    order_in_rest = (lax.broadcasted_iota(jnp.int32, (128, 256), 0) % 8) // REM

    def ffn(f, carry):
        cc, j = f // CHUNKS, f % CHUNKS

        @pl.when((dist > 0) | (f % 2 != c))
        def _():
            sib_copy(hs, f, share).wait_recv()

        at_k = pl.ds(pl.multiple_of(((j % 8) // 2) * 512, 512), 512)
        at_n = pl.ds(pl.multiple_of((j % 2) * 256, 256), 256)
        at_o = pl.ds(pl.multiple_of((j % 8) * 256, 256), 256)
        for h in range(2):
            at_r = pl.ds(pl.multiple_of(cc * 32 + h * MAIN, MAIN), MAIN)

            def product(h=h, at_r=at_r):
                rows = jnp.concatenate([rm[:, at_r, at_k].reshape(256, 512), rx[:, at_k]], axis=0)
                return jnp.dot(rows, w[h, cc, j], preferred_element_type=f32)

            @pl.when(j < 8)
            def _(h=h):
                hg[h, :, at_n] += product()

            @pl.when((j >= 8) & (j < 16))
            def _(h=h):
                hu[h, :, at_n] += product()

            @pl.when(j == 15)
            def _(h=h):
                gate = hg[h]
                inner[h] = (jax.nn.silu(gate) * hu[h]).astype(bf16)
                hg[h] = jnp.zeros_like(gate)
                hu[h] = jnp.zeros_like(gate)

            @pl.when(j >= 16)
            def _(h=h, at_r=at_r):
                rows = jnp.dot(inner[h], w[h, cc, j], preferred_element_type=f32)
                rm[:, at_r, at_o] = rows[:256].astype(bf16).reshape(16, MAIN, 256)
                mine = order_in_rest == cc * 2 + h
                orx[:, at_o] = jnp.where(mine, rows[256:], orx[:, at_o])

        return carry

    def activate(b):
        rows = pl.ds(pl.multiple_of(b * 128, 128), 128)
        center = to_column(stats[pl.ds(b, 1), :], 128) / CONV
        spread = to_column(stats[pl.ds(8 + b, 1), :], 128) / CONV - center * center
        normed = (filt[rows, :] - center) * lax.rsqrt(spread + 1e-05) * gain_c[:, my_cols] + shift_c[
            :, my_cols
        ]
        act[rows, :] = jax.nn.silu(normed).astype(bf16)

    def phase0(p, carry):
        step(p)
        activate(p - START)
        return lax.fori_loop(3 * (p - START), 3 * (p - START) + 3, ffn, carry)

    with jax.named_scope("s_phase0"):
        lax.fori_loop(START, START + 8, phase0, 0)

    def back(k):
        block, peer = block_at(k, -1)
        return pltpu.make_async_remote_copy(
            src_ref=rm.at[block, pl.ds(0, 32)], dst_ref=bm.at[me, pl.ds(0, 32)],
            send_sem=r_sent.at[k], recv_sem=r_recv.at[k], device_id=peer, device_id_type=MESH,
        )

    with jax.named_scope("s_back0"):
        for k in (1, 3, 2):
            act_copy(k).start()
        acts[y] = act[my_cols, :]
        for k in range(15):
            back(k).start()
        bm[me, 0:32] = rm[me, 0:32]

    def conv_part(q):
        at = pl.ds(pl.multiple_of(q * 512, 512), 512)
        total = None
        for b in range(4):
            term = jnp.dot(acts[b], cw[b, :, at], preferred_element_type=f32).astype(bf16).astype(f32)
            total = term if total is None else total + term
        conv_out[:, at] = total.astype(bf16)

    def phase1(p, carry):
        step(p)

        @pl.when(p == START + 9)
        def _():
            for k in (1, 3, 2):
                cw_copy(k).wait_recv()
                cs_copy(k).start()

        @pl.when(p == START + 11)
        def _():
            for k in (1, 3, 2):
                act_copy(k).wait_recv()
                cs_copy(k).wait_recv()

        @pl.when((p >= START + 12) & (p < START + 16))
        def _():
            conv_part(p - START - 12)

        low = jnp.where(p < START + 11, CHUNKS + 2 * (p - START - 8), p - FAR)
        high = jnp.where(p < START + 11, low + 2, low + 1)
        lax.fori_loop(low, high, ffn, 0)
        return carry

    def quarter(k, q, main):
        block, peer = block_at(k, -1)
        at = pl.ds(q * 512, 512)
        if main:
            src, dst = rm.at[block, pl.ds(32, 32), at], bm.at[me, pl.ds(32, 32), at]
        else:
            src, dst = rr.at[block, :, at], br.at[me, :, at]
        return pltpu.make_async_remote_copy(
            src_ref=src, dst_ref=dst, send_sem=q_sent.at[q, 1 - main, k],
            recv_sem=q_recv.at[q, 1 - main, k], device_id=peer, device_id_type=MESH,
        )

    with jax.named_scope("s_phase1"):
        last = TOTAL + FAR

        def tail(p, carry):
            phase1(p, carry)
            for q in range(4):

                @pl.when(p == last - 7 + 2 * q)
                def _(q=q):
                    at = slice(q * 512, q * 512 + 512)
                    rr[:, :, at] = orx[:, at].reshape(16, 8, 512).astype(bf16)
                    for main in (1, 0):
                        for k in range(15):
                            quarter(k, q, main).start()
                    bm[me, 32:64, at] = rm[me, 32:64, at]
                    br[me, :, at] = rr[me, :, at]

            return carry

        lax.fori_loop(START + 8, last, tail, 0)

    with jax.named_scope("s_combine0"):
        slot0_c, slot1_c = to_column(slot0, tokens), to_column(slot1, tokens)
        group = jax.nn.sigmoid(table[2:3, :])
        weight0 = to_column(group * jax.nn.sigmoid(table[3:4, :]), tokens)
        weight1 = to_column(group * jax.nn.sigmoid(-table[3:4, :]), tokens)

        def chosen(slot, cc):
            at = lax.broadcasted_iota(jnp.int32, (tokens, 512), 1)
            main = ((at // 32) * 64 + cc * 32 + at % 32).astype(f32)
            hits = jnp.where(main == slot, 1.0, 0.0).astype(bf16)
            if cc == 0:
                return hits
            rest = (lax.broadcasted_iota(jnp.int32, (tokens, 128), 1) + 1024).astype(f32)
            return jnp.concatenate([hits, jnp.where(rest == slot, 1.0, 0.0).astype(bf16)], axis=1)

        for k in range(15):
            back(k).wait_recv()
        pick0, pick1 = chosen(slot0_c, 0), chosen(slot1_c, 0)

        def combine0(q, carry):
            at = pl.ds(pl.multiple_of(q * 512, 512), 512)
            rows = bm[:, 0:32, at].reshape(512, 512)
            acc[:, at] = weight0 * jnp.dot(
                pick0, rows, preferred_element_type=f32
            ) + weight1 * jnp.dot(pick1, rows, preferred_element_type=f32)
            return carry

        lax.fori_loop(0, 4, combine0, 0)

    with jax.named_scope("s_combine1"):
        pick0b, pick1b = chosen(slot0_c, 1), chosen(slot1_c, 1)
        for q in range(4):
            for main in (1, 0):
                for k in range(15):
                    quarter(k, q, main).wait_recv()
            at = slice(q * 512, q * 512 + 512)
            rest = br[:, :, at].astype(f32).reshape(128, 512).astype(bf16)
            rows = jnp.concatenate([bm[:, 32:64, at].reshape(512, 512), rest], axis=0)
            total = acc[:, at] + (
                weight0 * jnp.dot(pick0b, rows, preferred_element_type=f32)
                + weight1 * jnp.dot(pick1b, rows, preferred_element_type=f32)
            )
            out[:, at] = total.astype(bf16)

    with jax.named_scope("s_sent"):
        halo.wait_send()
        for k in (1, 3, 2):
            stat_copy(k).wait_send()
            act_copy(k).wait_send()
            cw_copy(k).wait_send()
            cs_copy(k).wait_send()
        for k in range(15):
            for part in range(3):
                dispatch(k, part).wait_send()
            back(k).wait_send()
            for q in range(4):
                for main in (1, 0):
                    quarter(k, q, main).wait_send()

        def sent(n, carry):
            @pl.when((dist < 3) | (n % 2 == c))
            def _():
                ring_copy(n, avail).wait_send()

            sib_copy(hs, n, share).wait_send()
            return carry

        lax.fori_loop(0, TOTAL, sent, 0)


def on_device(
    conv_value,
    conv_gate,
    depth_weight,
    norm_gain,
    norm_shift,
    conv_out_weight,
    moe_input,
    moe_gain,
    route_experts,
    route_scores,
    expert_gate,
    expert_up,
    expert_down,
):
    bf16, f32 = jnp.bfloat16, jnp.float32
    rows, width = moe_input.shape
    span, channels = conv_value.shape
    table = jnp.concatenate([route_experts.T.astype(f32), route_scores.T], axis=0)
    hbm = pl.BlockSpec(memory_space=pl.ANY)
    vmem = pl.BlockSpec(memory_space=pltpu.VMEM)
    dma = pltpu.SemaphoreType.DMA
    return pl.pallas_call(
        kernel,
        out_shape=(
            jax.ShapeDtypeStruct((span // NY, width), bf16),
            jax.ShapeDtypeStruct((rows, width), bf16),
        ),
        in_specs=[hbm, hbm, hbm, vmem, vmem, hbm, hbm, vmem, vmem, hbm, hbm, hbm],
        out_specs=(vmem, vmem),
        scratch_shapes=[
            pltpu.VMEM((2, 2, CHUNKS, 512, 256), bf16),
            pltpu.VMEM((rows, width), bf16),
            pltpu.VMEM((16, 64, width), bf16),
            pltpu.VMEM((16, 8, width), bf16),
            pltpu.VMEM((16, 64, width), bf16),
            pltpu.VMEM((16, 8, width), bf16),
            pltpu.VMEM((16, 64, width), bf16),
            pltpu.VMEM((16, 8, width), bf16),
            pltpu.VMEM((2, 384, 512), f32),
            pltpu.VMEM((2, 384, 512), f32),
            pltpu.VMEM((2, 384, 512), bf16),
            pltpu.VMEM((128, width), bf16),
            pltpu.VMEM((128, width), f32),
            pltpu.VMEM((rows, width), f32),
            pltpu.VMEM((span, channels), bf16),
            pltpu.VMEM((span, channels), bf16),
            pltpu.VMEM((KERNEL, channels), f32),
            pltpu.VMEM((HALO + span, channels), f32),
            pltpu.VMEM((span, channels), f32),
            pltpu.VMEM((span, channels), bf16),
            pltpu.VMEM((NY, span // NY, channels), bf16),
            pltpu.VMEM((NY, channels, width), bf16),
            pltpu.VMEM((128 + HALO, channels), f32),
            pltpu.VMEM((HALO, channels), bf16),
            pltpu.VMEM((HALO, channels), bf16),
            pltpu.VMEM((NY, 16, 128), f32),
            pltpu.VMEM((16, 128), f32),
            dma((5,)),
            dma((TOTAL,)),
            dma((TOTAL,)),
            dma((TOTAL,)),
            dma,
            dma,
            dma((3, 15)),
            dma((3, 15)),
            dma((15,)),
            dma((15,)),
            dma((4, 2, 15)),
            dma((4, 2, 15)),
            dma((2,)),
            dma((4,)),
            dma((4,)),
            dma((4,)),
            dma((4,)),
            dma((4,)),
            dma((4,)),
            dma((4,)),
            dma((4,)),
        ],
        compiler_params=pltpu.CompilerParams(
            collective_id=0, has_side_effects=True, vmem_limit_bytes=67_000_000
        ),
        name="both",
    )(
        conv_value,
        conv_gate,
        depth_weight,
        norm_gain.reshape(1, CONV),
        norm_shift.reshape(1, CONV),
        conv_out_weight,
        moe_input,
        moe_gain.reshape(1, width),
        table,
        expert_gate,
        expert_up,
        expert_down,
    )


def solution(mesh):
    in_specs = (
        P("ep", "tp"),
        P("ep", "tp"),
        P(),
        P(),
        P(),
        P("tp", None),
        P(("ep", "tp"), None),
        P(),
        P(("ep", "tp"), None),
        P(("ep", "tp"), None),
        P("ep", None, None),
        P("ep", None, None),
        P("ep", None, None),
    )
    out_specs = (P(("ep", "tp"), None), P(("ep", "tp"), None))
    return jax.shard_map(
        on_device, mesh=mesh, in_specs=in_specs, out_specs=out_specs, check_vma=False
    )
```

time: 424 us -> 211 us (0.50)
  waiting for transfers between devices: 254 us -> 0 us
  Pallas kernels: 0 us -> 204 us
  local copies, waits for them, and re-layouts: 83.2 us -> 3.57 us
  matrix products: 22.7 us -> 0 us
  starting transfers between devices: 20.4 us -> 0 us
  other arithmetic: 17.3 us -> 1.97 us
  between operations: 14.3 us -> 0.65 us
  blocking collectives: 11.1 us -> 0 us
    all_to_all x2 -> x0, waiting for transfers between devices: 254 us -> none  [the longest x1 136 us: moe_half(): lax.all_to_all(send_buffer, 'ep', split_axis=0, concat_axis=0, tiled=True)]
    pallas_call x0 -> x1, Pallas kernels: none -> 204 us  [on_device(): pl.pallas_call(kernel, out_shape=(jax.ShapeDtypeStruct((span // NY, width...]
    reshape x5 -> x0, local copies, waits for them, and re-layouts: 36.7 us -> none  [the longest x1 7.77 us: moe_half(): flat_rows = arrived.reshape(-1, model_width)]
    dot_general x3 -> x0, matrix products: 22.7 us -> none  [the longest x1 11 us: moe_half(): jnp.dot(inner, expert_down[0], preferred_element_type=jnp.float32)]
    gather x2 -> x0, local copies, waits for them, and re-layouts: 22.3 us -> none  [the longest x1 12.3 us: moe_half(): padded_in[slot_token].reshape(experts_all, capacity, model_width)]
    all_to_all x2 -> x0, starting transfers between devices: 18.1 us -> none  [the longest x1 12.3 us: moe_half(): lax.all_to_all(send_buffer, 'ep', split_axis=0, concat_axis=0, tiled=True)]
    psum x1 -> x0, blocking collectives: 11.1 us -> none  [conv_half(): lax.psum((jnp.sum(filtered, axis=1), jnp.sum(filtered * filtered, axis=1)...]
    slice x5 -> x0, local copies, waits for them, and re-layouts: 10.5 us -> none  [the longest x1 7.93 us: moe_half(): picked[:, 0].astype(jnp.float32)]
  transfers between devices with their start and end apart: 4 -> 0, of which waited for: 2 -> 0; matrix products, arithmetic and copies ran while one was open for 21% -> 0% of each run, Pallas kernels for 0% -> 0%
where the time goes in v2:
time: 211 us; the launch traced here: 210 us
  Pallas kernels  204 us (97%)
  local copies, waits for them, and re-layouts  3.57 us (2%)
    pallas_call x1, Pallas kernels, on_device(): pl.pallas_call(kernel, out_shape=(jax.ShapeDtypeStruct((span // NY, width...  204 us

profile of v2, /device:TPU:2, one launch (start us, length us, event | category | flops | bytes accessed | tf_op | source)
XLA Modules:
  0.0 210.1 jit_solution(7524699167628715586)
XLA Ops:
  0.6 0.7 convert_bitcast_fusion
  1.3 1.3 pad_maximum_fusion.table
  2.6 203.9 %both.1 = (bf16[256,2048]{1,0:T(8,128)(2,1)}, bf16[384,2048]{1,0:T(8,128)(2,1)}) custom-call(bf16[1024,256]{1,0:T(8,128)(2,1)} %value_hbm.1, bf16[1024,256]{1,0:T(8,128)(2,1)} %gate_hbm.1, f32[31,1024]{1,0:T(8,128)} %taps_hbm.1, f32[1,1024]{1,0:T(1,128)} %bitcast.7, f32[1,1024]{1,0:T(1,128)} %bitcast.8, bf16[256,2048]{1,0:T(8,128)(2,1)} %cw_hbm.1, ...), custom_call_target="tpu_custom_call" | custom-call | tf_op jit(solution)/shard_map/both/pallas_call | solution.py:576
  206.5 0.0 copy-start
  206.5 2.4 %copy.17 = bf16[256,2048]{1,0:T(8,128)(2,1)} copy(bf16[256,2048]{1,0:T(8,128)(2,1)} %get-tuple-element.4) | data formatting | bytes 2097152
  208.9 0.0 copy-done
  208.9 1.1 copy.18
Async XLA Ops:
  206.5 2.4 %copy-start = (bf16[384,2048]{1,0:T(8,128)(2,1)S(1)}, bf16[384,2048]{1,0:T(8,128)(2,1)}, u32[]{:S(2)}) copy-start(bf16[384,2048]{1,0:T(8,128)(2,1)} %get-tuple-element.5) | copy-start | bytes 4718596

commit v3 on v2

--- a/solution.py
+++ b/solution.py
@@ -12,21 +12,31 @@
 HALO = 32
 MAIN = 16
 REM = 2
-CHUNKS = 24
+PIECE = 256
+CHUNKS = 48
 TOTAL = 2 * CHUNKS
-HOP = 2
-FAR = 4 * HOP + 1
-START = 28
+HOP = 4
+FAR = 3 * HOP + 3
+OUTER = 4 * HOP + 2
+START = 50
+MIDDLE = START + 16
+LAST = TOTAL + FAR
 OFFSETS = [
     (1, 0), (3, 0), (0, 1), (0, 3), (1, 1), (3, 3), (1, 3), (3, 1),
     (2, 0), (0, 2), (2, 2), (1, 2), (3, 2), (2, 1), (2, 3),
 ]
 
 
-def slot_of(expert, rank):
+def slot_of(expert, rank, z, c):
     high = expert // 8
-    block = ((expert // 2) % 4) * NY + high % 4
-    order = (expert % 2) * 2 + high // 4
+    yy = high % 4
+    block = ((expert // 2) % 4) * NY + yy
+    hops = (z - yy + 8) % 4
+    below = ((z - hops - yy + 8) % 8) // 4
+    other = jnp.where(high // 4 == below, 0, 1)
+    flip = (other + jnp.where(hops == 0, c, 0)) % 2
+    half = jnp.where(flip == 0, expert % 2, 1 - expert % 2)
+    order = half * 2 + other
     main = (block * 64 + order * MAIN).astype(jnp.float32) + rank
     rest = (1024 + block * 8 + order * REM).astype(jnp.float32) + (rank - MAIN)
     return jnp.where(rank < MAIN, main, jnp.where(rank < MAIN + REM, rest, -1.0))
@@ -50,10 +60,10 @@
 
 def kernel(
     value_hbm, gate_hbm, taps_hbm, gain_c, shift_c, cw_hbm,
-    x_hbm, gain, table, wg_hbm, wu_hbm, wd_hbm,
+    x_hbm, gain, experts, scores, wg_hbm, wu_hbm, wd_hbm,
     conv_out, out,
-    w, xn, sm, sr, rm, rr, bm, br, hg, hu, inner, rx, orx, acc,
-    val, gat, taps, pad, filt, act, acts, cw, window, halo_out, halo_in, stat, stats,
+    w, xn, sm, sr, rm, rr, bm, br, hidden, inner, rx, orx,
+    val, gat, taps, pad, acts, cw, window, halo_out, halo_in, stat, stats,
     load, avail, share, foreign, ring_sent, sib_sent,
     d_sent, d_recv, r_sent, r_recv, q_sent, q_recv,
     halo_sem, stat_sent, stat_recv, act_sent, act_recv, cw_sent, cw_recv, cs_sent, cs_recv,
@@ -86,79 +96,75 @@
 
     @pl.when(dist == 0)
     def _():
-        for part, ref in enumerate((wg_hbm, wu_hbm)):
-            for j in range(8):
-                pltpu.make_async_copy(
-                    ref.at[0, pl.ds((j // 2) * 512, 512), pl.ds((j % 2) * 256, 256)],
-                    w.at[hs, c, part * 8 + j],
-                    avail.at[c * CHUNKS + part * 8 + j],
-                ).start()
-        for j in range(8):
-            pltpu.make_async_copy(
-                wd_hbm.at[0, :, pl.ds(j * 256, 256)],
-                w.at[hs, c, 16 + j],
-                avail.at[c * CHUNKS + 16 + j],
-            ).start()
+        def native(i, src):
+            dst = w.at[hs, c, pl.ds(i * PIECE, PIECE)]
+            pltpu.make_async_copy(src, dst, avail.at[c * CHUNKS + i]).start()
+
+        for i in range(CHUNKS):
+            ref = wg_hbm if i < 16 else wu_hbm if i < 32 else wd_hbm
+            block, row = (i // 8 % 2, i % 8) if i < 32 else ((i - 32) // 2, i % 2)
+            native(i, ref.at[0, pl.ds(row * PIECE, PIECE), pl.ds(block * 256, 256)])
 
     for copy in loads:
         copy.start()
 
-    with jax.named_scope("s_barrier"):
-        barrier = pltpu.get_barrier_semaphore()
-        peers = [(device(z, (x + dx) % NX, c), (y + dy) % NY) for dx, dy in OFFSETS]
-        peers += [(device((z + 1) % NZ, x, c), y), (device((z + NZ - 1) % NZ, x, c), y), sibling]
-        peers += [((ep + 1) % 64, y), ((ep + 63) % 64, y)]
-        for peer in peers:
-            pl.semaphore_signal(barrier, inc=1, device_id=peer, device_id_type=MESH)
-        pl.semaphore_wait(barrier, len(peers))
+    barrier = pltpu.get_barrier_semaphore()
+    peers = [(device(z, (x + dx) % NX, c), (y + dy) % NY) for dx, dy in OFFSETS]
+    peers += [(device((z + 1) % NZ, x, c), y), (device((z + NZ - 1) % NZ, x, c), y), sibling]
+    peers += [((ep + 1) % 64, y), ((ep + 63) % 64, y)]
+    for peer in peers:
+        pl.semaphore_signal(barrier, inc=1, device_id=peer, device_id_type=MESH)
 
     def ring_copy(n, sem):
-        ref = w.at[hs, n // CHUNKS, n % CHUNKS]
+        ref = w.at[hs, n // CHUNKS, pl.ds(pl.multiple_of(n % CHUNKS * PIECE, PIECE), PIECE)]
         return pltpu.make_async_remote_copy(
             src_ref=ref, dst_ref=ref, send_sem=ring_sent, recv_sem=sem.at[n],
             device_id=ring_to, device_id_type=MESH,
         )
 
     def sib_copy(h, n, sem):
-        ref = w.at[h, n // CHUNKS, n % CHUNKS]
+        ref = w.at[h, n // CHUNKS, pl.ds(pl.multiple_of(n % CHUNKS * PIECE, PIECE), PIECE)]
         return pltpu.make_async_remote_copy(
             src_ref=ref, dst_ref=ref, send_sem=sib_sent, recv_sem=sem.at[n],
             device_id=sibling, device_id_type=MESH,
         )
 
+    def expert_at(n):
+        return jnp.where(c == 0, n, (n + CHUNKS) % TOTAL)
+
     def own(n):
-        ring_copy(n, avail).wait_recv()
+        i = expert_at(n)
+        ring_copy(i, avail).wait_recv()
 
         @pl.when(dist < 3)
         def _():
-            ring_copy(n, avail).start()
-
-        @pl.when((dist == 3) & (n % 2 == c))
-        def _():
-            ring_copy(n, foreign).start()
+            ring_copy(i, avail).start()
+
+        @pl.when((dist == 3) & (n < CHUNKS))
+        def _():
+            ring_copy(i, foreign).start()
 
         @pl.when(dist > 0)
         def _():
-            sib_copy(hs, n, share).start()
-
-        @pl.when((dist == 0) & (n // CHUNKS == c))
-        def _():
-            sib_copy(hs, n, avail).start()
+            sib_copy(hs, i, share).start()
+
+        @pl.when((dist == 0) & (i // CHUNKS == c))
+        def _():
+            sib_copy(hs, i, avail).start()
 
     def step(p):
         n = p - HOP * dist
-        m = p - FAR
+        m = p - OUTER
 
         @pl.when((n >= 0) & (n < TOTAL))
         def _():
             own(n)
 
-        @pl.when((dist == 0) & (m >= 0) & (m < TOTAL) & (m % 2 == c))
-        def _():
-            ring_copy(m, foreign).wait_recv()
-            sib_copy(1 - hs, m, share).start()
-
-    step(0)
+        @pl.when((dist == 0) & (m >= 0) & (m < CHUNKS))
+        def _():
+            i = expert_at(m)
+            ring_copy(i, foreign).wait_recv()
+            sib_copy(1 - hs, i, share).start()
 
     with jax.named_scope("s_gated"):
         loads[0].wait()
@@ -172,17 +178,14 @@
 
         lax.fori_loop(0, 8, gated, 0)
         halo_out[...] = pad[1024 : 1024 + HALO, :].astype(bf16)
+
         halo = pltpu.make_async_remote_copy(
             src_ref=halo_out, dst_ref=halo_in, send_sem=halo_sem.at[0], recv_sem=halo_sem.at[1],
             device_id=((ep + 1) % 64, y), device_id_type=MESH,
         )
-        halo.start()
-
-    step(1)
-
     with jax.named_scope("s_route"):
         tokens = xn.shape[0]
-        first, second = table[0:1, :].astype(jnp.int32), table[1:2, :].astype(jnp.int32)
+        first, second = experts[0:1, :], experts[1:2, :]
         ids = lax.broadcasted_iota(jnp.int32, (64, tokens), 0)
         hit0, hit1 = ids == first, ids == second
         both = jnp.where(hit0 | hit1, 1.0, 0.0).astype(bf16)
@@ -190,8 +193,8 @@
         col_t = lax.broadcasted_iota(jnp.int32, (tokens, tokens), 1)
         earlier = jnp.where(row_t < col_t, 1.0, 0.0).astype(bf16)
         counts = jnp.dot(both, earlier, preferred_element_type=f32)
-        slot0 = slot_of(first, jnp.sum(jnp.where(hit0, counts, 0.0), axis=0, keepdims=True))
-        slot1 = slot_of(second, jnp.sum(jnp.where(hit1, counts, 0.0), axis=0, keepdims=True))
+        slot0 = slot_of(first, jnp.sum(jnp.where(hit0, counts, 0.0), axis=0, keepdims=True), z, c)
+        slot1 = slot_of(second, jnp.sum(jnp.where(hit1, counts, 0.0), axis=0, keepdims=True), z, c)
 
     with jax.named_scope("s_norm"):
         loads[2].wait()
@@ -204,7 +207,11 @@
             return carry
 
         lax.fori_loop(0, 6, norm, 0)
-    step(2)
+
+    with jax.named_scope("s_barrier"):
+        pl.semaphore_wait(barrier, len(peers))
+    halo.start()
+    step(0)
 
     def picked(base, count):
         at = (lax.broadcasted_iota(jnp.int32, (count, tokens), 0) + base).astype(f32)
@@ -221,10 +228,7 @@
 
         lax.fori_loop(0, 4, cols, 0)
 
-        @pl.when(g % 2 == 1)
-        def _():
-            step(3 + g // 2)
-
+        step(1 + g)
         return carry
 
     with jax.named_scope("s_gather"):
@@ -268,7 +272,8 @@
         loads[3].wait()
 
         def filter_block(b, carry):
-            step(5 + b)
+            step(5 + 2 * b)
+            step(6 + 2 * b)
             base = pl.multiple_of(b * 128, 128)
             window[...] = pad[pl.ds(base, 128 + HALO), :]
             total = None
@@ -276,7 +281,7 @@
                 low = HALO - KERNEL + 1 + k
                 term = taps[k : k + 1, :] * window[low : low + 128, :]
                 total = term if total is None else total + term
-            filt[pl.ds(base, 128), :] = total
+            pad[pl.ds(base, 128), :] = total
             stat[y, pl.ds(b, 1), :] = to_row(jnp.sum(total, axis=1, keepdims=True))
             stat[y, pl.ds(8 + b, 1), :] = to_row(jnp.sum(total * total, axis=1, keepdims=True))
             return carry
@@ -296,7 +301,7 @@
     def act_copy(k):
         yy, peer = near(k)
         return pltpu.make_async_remote_copy(
-            src_ref=act.at[pl.ds(pl.multiple_of(yy * 256, 256), 256)], dst_ref=acts.at[y],
+            src_ref=val.at[pl.ds(pl.multiple_of(yy * 256, 256), 256)], dst_ref=acts.at[y],
             send_sem=act_sent.at[k], recv_sem=act_recv.at[k], device_id=peer, device_id_type=MESH,
         )
 
@@ -326,15 +331,13 @@
         return carry
 
     with jax.named_scope("s_pumps"):
-        lax.fori_loop(13, START, only_step, 0)
+        lax.fori_loop(21, START, only_step, 0)
 
     with jax.named_scope("s_wait_rows"):
         for part in range(3):
             for k in range(15):
                 dispatch(k, part).wait_recv()
         rx[...] = rr[...].astype(f32).reshape(128, 2048).astype(bf16)
-        hg[...] = jnp.zeros_like(hg)
-        hu[...] = jnp.zeros_like(hu)
 
     with jax.named_scope("s_wait_stat"):
         for k in (1, 3, 2):
@@ -343,63 +346,81 @@
 
     order_in_rest = (lax.broadcasted_iota(jnp.int32, (128, 256), 0) % 8) // REM
 
-    def ffn(f, carry):
-        cc, j = f // CHUNKS, f % CHUNKS
-
-        @pl.when((dist > 0) | (f % 2 != c))
-        def _():
-            sib_copy(hs, f, share).wait_recv()
-
-        at_k = pl.ds(pl.multiple_of(((j % 8) // 2) * 512, 512), 512)
-        at_n = pl.ds(pl.multiple_of((j % 2) * 256, 256), 256)
-        at_o = pl.ds(pl.multiple_of((j % 8) * 256, 256), 256)
-        for h in range(2):
-            at_r = pl.ds(pl.multiple_of(cc * 32 + h * MAIN, MAIN), MAIN)
-
-            def product(h=h, at_r=at_r):
-                rows = jnp.concatenate([rm[:, at_r, at_k].reshape(256, 512), rx[:, at_k]], axis=0)
-                return jnp.dot(rows, w[h, cc, j], preferred_element_type=f32)
-
-            @pl.when(j < 8)
-            def _(h=h):
-                hg[h, :, at_n] += product()
-
-            @pl.when((j >= 8) & (j < 16))
-            def _(h=h):
-                hu[h, :, at_n] += product()
-
-            @pl.when(j == 15)
-            def _(h=h):
-                gate = hg[h]
-                inner[h] = (jax.nn.silu(gate) * hu[h]).astype(bf16)
-                hg[h] = jnp.zeros_like(gate)
-                hu[h] = jnp.zeros_like(gate)
-
-            @pl.when(j >= 16)
-            def _(h=h, at_r=at_r):
-                rows = jnp.dot(inner[h], w[h, cc, j], preferred_element_type=f32)
-                rm[:, at_r, at_o] = rows[:256].astype(bf16).reshape(16, MAIN, 256)
-                mine = order_in_rest == cc * 2 + h
-                orx[:, at_o] = jnp.where(mine, rows[256:], orx[:, at_o])
-
-        return carry
+    def of_half(half, s):
+        e_low = jnp.where((dist == 0) & (c == 1), 1 - half, half)
+        return jnp.where(s == 0, h_low, 1 - h_low), jnp.where(s == 0, e_low, 1 - e_low)
+
+    def shared(half, low, count):
+        others = jnp.where(dist == 0, 1 - c, jnp.where(c == 0, 1 - half, half))
+
+        def wait(i, carry):
+            sib_copy(hs, others * CHUNKS + i, share).wait_recv()
+            return carry
+
+        @pl.when((dist > 0) | (half == 0))
+        def _():
+            lax.fori_loop(low, low + count, wait, 0)
+
+    def rows_at(half, s):
+        return pl.ds(pl.multiple_of(half * 32 + s * MAIN, MAIN), MAIN)
+
+    def gate_up(half, block, s):
+        @pl.when(s == 0)
+        def _():
+            shared(half, block * 8, 8)
+
+        h, e = of_half(half, s)
+        rows = jnp.concatenate([rm[:, rows_at(half, s), :].reshape(256, 2048), rx[...]], axis=0)
+        weight = w[h, e, pl.ds(pl.multiple_of(block * 2048, 2048), 2048), :]
+        at = pl.ds(pl.multiple_of(block * 256, 256), 256)
+        hidden[s, :, at] = jnp.dot(rows, weight, preferred_element_type=f32)
+
+        @pl.when(block == 3)
+        def _():
+            inner[s] = (jax.nn.silu(hidden[s, :, 0:512]) * hidden[s, :, 512:1024]).astype(bf16)
+
+    def down(half, block):
+        shared(half, 32 + block * 2, 2)
+        at = pl.ds(pl.multiple_of(block * 256, 256), 256)
+        for s in range(2):
+            h, e = of_half(half, s)
+            weight = w[h, e, pl.ds(pl.multiple_of(8192 + block * 512, 512), 512), :]
+            rows = jnp.dot(inner[s], weight, preferred_element_type=f32)
+            rm[:, rows_at(half, s), at] = rows[:256].astype(bf16).reshape(16, MAIN, 256)
+            here = order_in_rest == half * 2 + s
+            orx[:, at] = jnp.where(here, rows[256:], orx[:, at])
 
     def activate(b):
         rows = pl.ds(pl.multiple_of(b * 128, 128), 128)
         center = to_column(stats[pl.ds(b, 1), :], 128) / CONV
         spread = to_column(stats[pl.ds(8 + b, 1), :], 128) / CONV - center * center
-        normed = (filt[rows, :] - center) * lax.rsqrt(spread + 1e-05) * gain_c[:, my_cols] + shift_c[
+        normed = (pad[rows, :] - center) * lax.rsqrt(spread + 1e-05) * gain_c[:, my_cols] + shift_c[
             :, my_cols
         ]
-        act[rows, :] = jax.nn.silu(normed).astype(bf16)
+        val[rows, :] = jax.nn.silu(normed).astype(bf16)
 
     def phase0(p, carry):
         step(p)
-        activate(p - START)
-        return lax.fori_loop(3 * (p - START), 3 * (p - START) + 3, ffn, carry)
+
+        @pl.when(p < START + 8)
+        def _():
+            activate(p - START)
+            gate_up(0, (p - START) // 2, (p - START) % 2)
+
+        @pl.when(p == START + 8)
+        def _():
+            for k in (1, 3, 2):
+                act_copy(k).start()
+            acts[y] = val[my_cols, :]
+
+        @pl.when(p >= START + 8)
+        def _():
+            down(0, p - START - 8)
+
+        return carry
 
     with jax.named_scope("s_phase0"):
-        lax.fori_loop(START, START + 8, phase0, 0)
+        lax.fori_loop(START, MIDDLE, phase0, 0)
 
     def back(k):
         block, peer = block_at(k, -1)
@@ -409,9 +430,6 @@
         )
 
     with jax.named_scope("s_back0"):
-        for k in (1, 3, 2):
-            act_copy(k).start()
-        acts[y] = act[my_cols, :]
         for k in range(15):
             back(k).start()
         bm[me, 0:32] = rm[me, 0:32]
@@ -424,28 +442,67 @@
             total = term if total is None else total + term
         conv_out[:, at] = total.astype(bf16)
 
+    slot0_c, slot1_c = to_column(slot0, tokens), to_column(slot1, tokens)
+    group = jax.nn.sigmoid(scores[0:1, :])
+    weight0 = to_column(group * jax.nn.sigmoid(scores[1:2, :]), tokens)
+    weight1 = to_column(group * jax.nn.sigmoid(-scores[1:2, :]), tokens)
+
+    def chosen(slot, half):
+        at = lax.broadcasted_iota(jnp.int32, (tokens, 512), 1)
+        main = ((at // 32) * 64 + half * 32 + at % 32).astype(f32)
+        hits = jnp.where(main == slot, 1.0, 0.0).astype(bf16)
+        if half == 0:
+            return hits
+        rest = (lax.broadcasted_iota(jnp.int32, (tokens, 128), 1) + 1024).astype(f32)
+        return jnp.concatenate([hits, jnp.where(rest == slot, 1.0, 0.0).astype(bf16)], axis=1)
+
+    def combine0(q):
+        at = pl.ds(pl.multiple_of(q * 512, 512), 512)
+        kept = pl.ds(pl.multiple_of(q % 2 * 512, 512), 512)
+        rows = bm[:, 0:32, at].reshape(512, 512)
+        pick0, pick1 = chosen(slot0_c, 0), chosen(slot1_c, 0)
+        hidden[q // 2, :, kept] = weight0 * jnp.dot(
+            pick0, rows, preferred_element_type=f32
+        ) + weight1 * jnp.dot(pick1, rows, preferred_element_type=f32)
+
     def phase1(p, carry):
         step(p)
 
-        @pl.when(p == START + 9)
+        @pl.when(p == MIDDLE + 2)
         def _():
             for k in (1, 3, 2):
                 cw_copy(k).wait_recv()
                 cs_copy(k).start()
 
-        @pl.when(p == START + 11)
+        @pl.when(p == MIDDLE + 6)
         def _():
             for k in (1, 3, 2):
                 act_copy(k).wait_recv()
                 cs_copy(k).wait_recv()
 
-        @pl.when((p >= START + 12) & (p < START + 16))
-        def _():
-            conv_part(p - START - 12)
-
-        low = jnp.where(p < START + 11, CHUNKS + 2 * (p - START - 8), p - FAR)
-        high = jnp.where(p < START + 11, low + 2, low + 1)
-        lax.fori_loop(low, high, ffn, 0)
+        @pl.when((p >= MIDDLE + 9) & (p < MIDDLE + 13))
+        def _():
+            conv_part(p - MIDDLE - 9)
+
+        ready = p - FAR - CHUNKS + 1
+
+        @pl.when((ready >= 8) & (ready < 34) & (ready % 8 < 2))
+        def _():
+            gate_up(1, ready // 8 - 1, ready % 8)
+
+        @pl.when((ready >= 34) & (ready % 2 == 0))
+        def _():
+            down(1, (ready - 34) // 2)
+
+        @pl.when(ready == 35)
+        def _():
+            for k in range(15):
+                back(k).wait_recv()
+
+        @pl.when((ready >= 35) & (ready % 2 == 1) & (ready < 43))
+        def _():
+            combine0((ready - 35) // 2)
+
         return carry
 
     def quarter(k, q, main):
@@ -461,13 +518,11 @@
         )
 
     with jax.named_scope("s_phase1"):
-        last = TOTAL + FAR
-
         def tail(p, carry):
             phase1(p, carry)
             for q in range(4):
 
-                @pl.when(p == last - 7 + 2 * q)
+                @pl.when(p == LAST - 13 + 4 * q)
                 def _(q=q):
                     at = slice(q * 512, q * 512 + 512)
                     rr[:, :, at] = orx[:, at].reshape(16, 8, 512).astype(bf16)
@@ -479,36 +534,7 @@
 
             return carry
 
-        lax.fori_loop(START + 8, last, tail, 0)
-
-    with jax.named_scope("s_combine0"):
-        slot0_c, slot1_c = to_column(slot0, tokens), to_column(slot1, tokens)
-        group = jax.nn.sigmoid(table[2:3, :])
-        weight0 = to_column(group * jax.nn.sigmoid(table[3:4, :]), tokens)
-        weight1 = to_column(group * jax.nn.sigmoid(-table[3:4, :]), tokens)
-
-        def chosen(slot, cc):
-            at = lax.broadcasted_iota(jnp.int32, (tokens, 512), 1)
-            main = ((at // 32) * 64 + cc * 32 + at % 32).astype(f32)
-            hits = jnp.where(main == slot, 1.0, 0.0).astype(bf16)
-            if cc == 0:
-                return hits
-            rest = (lax.broadcasted_iota(jnp.int32, (tokens, 128), 1) + 1024).astype(f32)
-            return jnp.concatenate([hits, jnp.where(rest == slot, 1.0, 0.0).astype(bf16)], axis=1)
-
-        for k in range(15):
-            back(k).wait_recv()
-        pick0, pick1 = chosen(slot0_c, 0), chosen(slot1_c, 0)
-
-        def combine0(q, carry):
-            at = pl.ds(pl.multiple_of(q * 512, 512), 512)
-            rows = bm[:, 0:32, at].reshape(512, 512)
-            acc[:, at] = weight0 * jnp.dot(
-                pick0, rows, preferred_element_type=f32
-            ) + weight1 * jnp.dot(pick1, rows, preferred_element_type=f32)
-            return carry
-
-        lax.fori_loop(0, 4, combine0, 0)
+        lax.fori_loop(MIDDLE, LAST, tail, 0)
 
     with jax.named_scope("s_combine1"):
         pick0b, pick1b = chosen(slot0_c, 1), chosen(slot1_c, 1)
@@ -519,7 +545,7 @@
             at = slice(q * 512, q * 512 + 512)
             rest = br[:, :, at].astype(f32).reshape(128, 512).astype(bf16)
             rows = jnp.concatenate([bm[:, 32:64, at].reshape(512, 512), rest], axis=0)
-            total = acc[:, at] + (
+            total = hidden[q // 2, :, q % 2 * 512 : q % 2 * 512 + 512] + (
                 weight0 * jnp.dot(pick0b, rows, preferred_element_type=f32)
                 + weight1 * jnp.dot(pick1b, rows, preferred_element_type=f32)
             )
@@ -541,7 +567,7 @@
                     quarter(k, q, main).wait_send()
 
         def sent(n, carry):
-            @pl.when((dist < 3) | (n % 2 == c))
+            @pl.when((dist < 3) | (n < CHUNKS))
             def _():
                 ring_copy(n, avail).wait_send()
 
@@ -569,7 +595,6 @@
     bf16, f32 = jnp.bfloat16, jnp.float32
     rows, width = moe_input.shape
     span, channels = conv_value.shape
-    table = jnp.concatenate([route_experts.T.astype(f32), route_scores.T], axis=0)
     hbm = pl.BlockSpec(memory_space=pl.ANY)
     vmem = pl.BlockSpec(memory_space=pltpu.VMEM)
     dma = pltpu.SemaphoreType.DMA
@@ -579,10 +604,10 @@
             jax.ShapeDtypeStruct((span // NY, width), bf16),
             jax.ShapeDtypeStruct((rows, width), bf16),
         ),
-        in_specs=[hbm, hbm, hbm, vmem, vmem, hbm, hbm, vmem, vmem, hbm, hbm, hbm],
+        in_specs=[hbm, hbm, hbm, vmem, vmem, hbm, hbm, vmem, vmem, vmem, hbm, hbm, hbm],
         out_specs=(vmem, vmem),
         scratch_shapes=[
-            pltpu.VMEM((2, 2, CHUNKS, 512, 256), bf16),
+            pltpu.VMEM((2, 2, CHUNKS * PIECE, 256), bf16),
             pltpu.VMEM((rows, width), bf16),
             pltpu.VMEM((16, 64, width), bf16),
             pltpu.VMEM((16, 8, width), bf16),
@@ -590,18 +615,14 @@
             pltpu.VMEM((16, 8, width), bf16),
             pltpu.VMEM((16, 64, width), bf16),
             pltpu.VMEM((16, 8, width), bf16),
-            pltpu.VMEM((2, 384, 512), f32),
-            pltpu.VMEM((2, 384, 512), f32),
+            pltpu.VMEM((2, 384, 1024), f32),
             pltpu.VMEM((2, 384, 512), bf16),
             pltpu.VMEM((128, width), bf16),
             pltpu.VMEM((128, width), f32),
-            pltpu.VMEM((rows, width), f32),
             pltpu.VMEM((span, channels), bf16),
             pltpu.VMEM((span, channels), bf16),
             pltpu.VMEM((KERNEL, channels), f32),
             pltpu.VMEM((HALO + span, channels), f32),
-            pltpu.VMEM((span, channels), f32),
-            pltpu.VMEM((span, channels), bf16),
             pltpu.VMEM((NY, span // NY, channels), bf16),
             pltpu.VMEM((NY, channels, width), bf16),
             pltpu.VMEM((128 + HALO, channels), f32),
@@ -644,7 +665,8 @@
         conv_out_weight,
         moe_input,
         moe_gain.reshape(1, width),
-        table,
+        route_experts.T,
+        route_scores.T,
         expert_gate,
         expert_up,
         expert_down,

time: 211 us -> 191 us (0.905)
  Pallas kernels: 204 us -> 185 us
    pallas_call x1, Pallas kernels: 204 us -> 185 us  [on_device(): pl.pallas_call(kernel, out_shape=(jax.ShapeDtypeStruct((span // NY, width...]
where the time goes in v3:
time: 191 us; the launch traced here: 190 us
  Pallas kernels  185 us (97%)
  local copies, waits for them, and re-layouts  3.57 us (2%)
    pallas_call x1, Pallas kernels, on_device(): pl.pallas_call(kernel, out_shape=(jax.ShapeDtypeStruct((span // NY, width...  185 us

profile of v3, /device:TPU:2, one launch (start us, length us, event | category | flops | bytes accessed | tf_op | source)
XLA Modules:
  0.0 189.6 jit_solution(6202024894221233156)
XLA Ops:
  0.6 185.3 %both.1 = (bf16[256,2048]{1,0:T(8,128)(2,1)}, bf16[384,2048]{1,0:T(8,128)(2,1)}) custom-call(bf16[1024,256]{1,0:T(8,128)(2,1)} %value_hbm.1, bf16[1024,256]{1,0:T(8,128)(2,1)} %gate_hbm.1, f32[31,1024]{1,0:T(8,128)} %taps_hbm.1, f32[1,1024]{1,0:T(1,128)} %bitcast.6, f32[1,1024]{1,0:T(1,128)} %bitcast.7, bf16[256,2048]{1,0:T(8,128)(2,1)} %cw_hbm.1, ...), custom_call_target="tpu_custom_call" | custom-call | tf_op jit(solution)/shard_map/both/pallas_call | solution.py:601
  186.0 0.0 copy-start
  186.0 2.4 %copy.17 = bf16[256,2048]{1,0:T(8,128)(2,1)} copy(bf16[256,2048]{1,0:T(8,128)(2,1)} %get-tuple-element.4) | data formatting | bytes 2097152
  188.4 0.0 copy-done
  188.4 1.1 copy.18
Async XLA Ops:
  186.0 2.4 %copy-start = (bf16[384,2048]{1,0:T(8,128)(2,1)S(1)}, bf16[384,2048]{1,0:T(8,128)(2,1)}, u32[]{:S(2)}) copy-start(bf16[384,2048]{1,0:T(8,128)(2,1)} %get-tuple-element.5) | copy-start | bytes 4718596

commit v4 on v3

--- a/solution.py
+++ b/solution.py
@@ -59,14 +59,15 @@
 
 
 def kernel(
-    value_hbm, gate_hbm, taps_hbm, gain_c, shift_c, cw_hbm,
-    x_hbm, gain, experts, scores, wg_hbm, wu_hbm, wd_hbm,
+    value_hbm, gate_hbm, taps_hbm, gain_c_hbm, shift_c_hbm, cw_hbm,
+    x_hbm, gain_hbm, experts_hbm, scores_hbm, wg_hbm, wu_hbm, wd_hbm,
     conv_out, out,
-    w, xn, sm, sr, rm, rr, bm, br, hidden, inner, rx, orx,
-    val, gat, taps, pad, acts, cw, window, halo_out, halo_in, stat, stats,
-    load, avail, share, foreign, ring_sent, sib_sent,
+    w, xn, sm, sr, rm, sx, bm, rest_out, rest_in, hidden, inner, rx, orx,
+    val, gat, taps, gain_c, shift_c, gain, experts, scores,
+    pad, acts, cw, window, halo_out, halo_in, stat, stats,
+    load, native, avail, share, ring_sent, sib_sent,
     d_sent, d_recv, r_sent, r_recv, q_sent, q_recv,
-    halo_sem, stat_sent, stat_recv, act_sent, act_recv, cw_sent, cw_recv, cs_sent, cs_recv,
+    halo_sem, stat_sem, act_sem, cw_sem, cs_sem,
 ):
     f32, bf16 = jnp.float32, jnp.bfloat16
     ep = lax.axis_index("ep")
@@ -92,18 +93,23 @@
         pltpu.make_async_copy(x_hbm, xn, load.at[2]),
         pltpu.make_async_copy(taps_hbm.at[:, my_cols], taps, load.at[3]),
         pltpu.make_async_copy(cw_hbm, cw.at[y], load.at[4]),
+        pltpu.make_async_copy(gain_c_hbm.at[:, my_cols], gain_c, load.at[5]),
+        pltpu.make_async_copy(shift_c_hbm.at[:, my_cols], shift_c, load.at[6]),
+        pltpu.make_async_copy(gain_hbm, gain, load.at[7]),
+        pltpu.make_async_copy(experts_hbm, experts, load.at[8]),
+        pltpu.make_async_copy(scores_hbm, scores, load.at[9]),
     ]
 
     @pl.when(dist == 0)
     def _():
-        def native(i, src):
-            dst = w.at[hs, c, pl.ds(i * PIECE, PIECE)]
-            pltpu.make_async_copy(src, dst, avail.at[c * CHUNKS + i]).start()
-
         for i in range(CHUNKS):
             ref = wg_hbm if i < 16 else wu_hbm if i < 32 else wd_hbm
             block, row = (i // 8 % 2, i % 8) if i < 32 else ((i - 32) // 2, i % 2)
-            native(i, ref.at[0, pl.ds(row * PIECE, PIECE), pl.ds(block * 256, 256)])
+            pltpu.make_async_copy(
+                ref.at[0, pl.ds(row * PIECE, PIECE), pl.ds(block * 256, 256)],
+                w.at[hs, c, pl.ds(i * PIECE, PIECE)],
+                native.at[i // 8],
+            ).start()
 
     for copy in loads:
         copy.start()
@@ -115,42 +121,54 @@
     for peer in peers:
         pl.semaphore_signal(barrier, inc=1, device_id=peer, device_id_type=MESH)
 
-    def ring_copy(n, sem):
-        ref = w.at[hs, n // CHUNKS, pl.ds(pl.multiple_of(n % CHUNKS * PIECE, PIECE), PIECE)]
-        return pltpu.make_async_remote_copy(
-            src_ref=ref, dst_ref=ref, send_sem=ring_sent, recv_sem=sem.at[n],
+    def arrived(ref, sem):
+        pltpu.make_async_copy(ref, ref, sem).wait()
+
+    def piece(h, i):
+        return w.at[h, i // CHUNKS, pl.ds(pl.multiple_of(i % CHUNKS * PIECE, PIECE), PIECE)]
+
+    def ring_copy(i):
+        return pltpu.make_async_remote_copy(
+            src_ref=piece(hs, i), dst_ref=piece(hs, i), send_sem=ring_sent, recv_sem=avail.at[i],
             device_id=ring_to, device_id_type=MESH,
         )
 
-    def sib_copy(h, n, sem):
-        ref = w.at[h, n // CHUNKS, pl.ds(pl.multiple_of(n % CHUNKS * PIECE, PIECE), PIECE)]
-        return pltpu.make_async_remote_copy(
-            src_ref=ref, dst_ref=ref, send_sem=sib_sent, recv_sem=sem.at[n],
+    def sib_copy(h, i, sem):
+        return pltpu.make_async_remote_copy(
+            src_ref=piece(h, i), dst_ref=piece(h, i), send_sem=sib_sent, recv_sem=sem,
             device_id=sibling, device_id_type=MESH,
         )
+
+    def share_of(i):
+        j = i % CHUNKS
+        return share.at[i // CHUNKS * 12 + jnp.where(j < 32, j // 8, 4 + (j - 32) // 2)]
 
     def expert_at(n):
         return jnp.where(c == 0, n, (n + CHUNKS) % TOTAL)
 
     def own(n):
         i = expert_at(n)
-        ring_copy(i, avail).wait_recv()
-
-        @pl.when(dist < 3)
-        def _():
-            ring_copy(i, avail).start()
-
-        @pl.when((dist == 3) & (n < CHUNKS))
-        def _():
-            ring_copy(i, foreign).start()
+        mine = (dist == 0) & (i // CHUNKS == c)
+
+        @pl.when(mine & (i % 8 == 0))
+        def _():
+            arrived(w.at[hs, c, pl.ds(0, 8 * PIECE)], native.at[i % CHUNKS // 8])
+
+        @pl.when(jnp.logical_not(mine))
+        def _():
+            ring_copy(i).wait_recv()
+
+        @pl.when((dist < 3) | (n < CHUNKS))
+        def _():
+            ring_copy(i).start()
 
         @pl.when(dist > 0)
         def _():
-            sib_copy(hs, i, share).start()
-
-        @pl.when((dist == 0) & (i // CHUNKS == c))
-        def _():
-            sib_copy(hs, i, avail).start()
+            sib_copy(hs, i, share_of(i)).start()
+
+        @pl.when(mine)
+        def _():
+            sib_copy(hs, i, avail.at[i]).start()
 
     def step(p):
         n = p - HOP * dist
@@ -163,8 +181,8 @@
         @pl.when((dist == 0) & (m >= 0) & (m < CHUNKS))
         def _():
             i = expert_at(m)
-            ring_copy(i, foreign).wait_recv()
-            sib_copy(1 - hs, i, share).start()
+            ring_copy(i).wait_recv()
+            sib_copy(1 - hs, i, share_of(i)).start()
 
     with jax.named_scope("s_gated"):
         loads[0].wait()
@@ -185,6 +203,8 @@
         )
     with jax.named_scope("s_route"):
         tokens = xn.shape[0]
+        loads[8].wait()
+        loads[9].wait()
         first, second = experts[0:1, :], experts[1:2, :]
         ids = lax.broadcasted_iota(jnp.int32, (64, tokens), 0)
         hit0, hit1 = ids == first, ids == second
@@ -198,6 +218,7 @@
 
     with jax.named_scope("s_norm"):
         loads[2].wait()
+        loads[7].wait()
 
         def norm(b, carry):
             rows = pl.ds(pl.multiple_of(b * 64, 64), 64)
@@ -253,9 +274,9 @@
         if part < 2:
             src, dst = sm.at[block, pl.ds(part * 32, 32)], rm.at[me, pl.ds(part * 32, 32)]
         else:
-            src, dst = sr.at[block], rr.at[me]
-        return pltpu.make_async_remote_copy(
-            src_ref=src, dst_ref=dst, send_sem=d_sent.at[part, k], recv_sem=d_recv.at[part, k],
+            src, dst = sr.at[block], sx.at[me]
+        return pltpu.make_async_remote_copy(
+            src_ref=src, dst_ref=dst, send_sem=d_sent.at[part // 2], recv_sem=d_recv.at[part],
             device_id=peer, device_id_type=MESH,
         )
 
@@ -264,7 +285,7 @@
             for k in range(15):
                 dispatch(k, part).start()
         rm[me] = sm[me]
-        rr[me] = sr[me]
+        sx[me] = sr[me]
 
     with jax.named_scope("s_filter"):
         halo.wait_recv()
@@ -294,7 +315,7 @@
 
     def stat_copy(k):
         return pltpu.make_async_remote_copy(
-            src_ref=stat.at[y], dst_ref=stat.at[y], send_sem=stat_sent.at[k], recv_sem=stat_recv.at[k],
+            src_ref=stat.at[y], dst_ref=stat.at[y], send_sem=stat_sem.at[0], recv_sem=stat_sem.at[1],
             device_id=near(k)[1], device_id_type=MESH,
         )
 
@@ -302,22 +323,22 @@
         yy, peer = near(k)
         return pltpu.make_async_remote_copy(
             src_ref=val.at[pl.ds(pl.multiple_of(yy * 256, 256), 256)], dst_ref=acts.at[y],
-            send_sem=act_sent.at[k], recv_sem=act_recv.at[k], device_id=peer, device_id_type=MESH,
+            send_sem=act_sem.at[0], recv_sem=act_sem.at[1], device_id=peer, device_id_type=MESH,
         )
 
     half = pl.ds(pl.multiple_of(c * 128, 128), 128)
 
     def cw_copy(k):
         return pltpu.make_async_remote_copy(
-            src_ref=cw.at[y, half], dst_ref=cw.at[y, half], send_sem=cw_sent.at[k],
-            recv_sem=cw_recv.at[k], device_id=near(k)[1], device_id_type=MESH,
+            src_ref=cw.at[y, half], dst_ref=cw.at[y, half], send_sem=cw_sem.at[0],
+            recv_sem=cw_sem.at[1], device_id=near(k)[1], device_id_type=MESH,
         )
 
     def cs_copy(k):
         yy = (y + NY - k) % NY
         return pltpu.make_async_remote_copy(
-            src_ref=cw.at[yy, half], dst_ref=cw.at[yy, half], send_sem=cs_sent.at[k],
-            recv_sem=cs_recv.at[k], device_id=sibling, device_id_type=MESH,
+            src_ref=cw.at[yy, half], dst_ref=cw.at[yy, half], send_sem=cs_sem.at[0],
+            recv_sem=cs_sem.at[1], device_id=sibling, device_id_type=MESH,
         )
 
     loads[4].wait()
@@ -334,14 +355,15 @@
         lax.fori_loop(21, START, only_step, 0)
 
     with jax.named_scope("s_wait_rows"):
-        for part in range(3):
-            for k in range(15):
-                dispatch(k, part).wait_recv()
-        rx[...] = rr[...].astype(f32).reshape(128, 2048).astype(bf16)
+        for part in range(2):
+            arrived(rm.at[pl.ds(0, 15), pl.ds(0, 32)], d_recv.at[part])
+        arrived(sx.at[pl.ds(0, 15)], d_recv.at[2])
+        rx[...] = sx[...].astype(f32).reshape(128, 2048).astype(bf16)
 
     with jax.named_scope("s_wait_stat"):
-        for k in (1, 3, 2):
-            stat_copy(k).wait_recv()
+        arrived(stat.at[pl.ds(0, 3)], stat_sem.at[1])
+        loads[5].wait()
+        loads[6].wait()
         stats[...] = (stat[0] + stat[1]) + (stat[2] + stat[3])
 
     order_in_rest = (lax.broadcasted_iota(jnp.int32, (128, 256), 0) % 8) // REM
@@ -353,13 +375,9 @@
     def shared(half, low, count):
         others = jnp.where(dist == 0, 1 - c, jnp.where(c == 0, 1 - half, half))
 
-        def wait(i, carry):
-            sib_copy(hs, others * CHUNKS + i, share).wait_recv()
-            return carry
-
         @pl.when((dist > 0) | (half == 0))
         def _():
-            lax.fori_loop(low, low + count, wait, 0)
+            arrived(w.at[hs, 0, pl.ds(0, count * PIECE)], share_of(others * CHUNKS + low))
 
     def rows_at(half, s):
         return pl.ds(pl.multiple_of(half * 32 + s * MAIN, MAIN), MAIN)
@@ -394,9 +412,7 @@
         rows = pl.ds(pl.multiple_of(b * 128, 128), 128)
         center = to_column(stats[pl.ds(b, 1), :], 128) / CONV
         spread = to_column(stats[pl.ds(8 + b, 1), :], 128) / CONV - center * center
-        normed = (pad[rows, :] - center) * lax.rsqrt(spread + 1e-05) * gain_c[:, my_cols] + shift_c[
-            :, my_cols
-        ]
+        normed = (pad[rows, :] - center) * lax.rsqrt(spread + 1e-05) * gain_c[...] + shift_c[...]
         val[rows, :] = jax.nn.silu(normed).astype(bf16)
 
     def phase0(p, carry):
@@ -422,17 +438,37 @@
     with jax.named_scope("s_phase0"):
         lax.fori_loop(START, MIDDLE, phase0, 0)
 
-    def back(k):
+    def back(k, main):
         block, peer = block_at(k, -1)
-        return pltpu.make_async_remote_copy(
-            src_ref=rm.at[block, pl.ds(0, 32)], dst_ref=bm.at[me, pl.ds(0, 32)],
-            send_sem=r_sent.at[k], recv_sem=r_recv.at[k], device_id=peer, device_id_type=MESH,
-        )
+        if main:
+            src, dst = rm.at[block, pl.ds(0, 32)], bm.at[me, pl.ds(0, 32)]
+        else:
+            src, dst = rest_out.at[0, block], rest_in.at[0, me]
+        return pltpu.make_async_remote_copy(
+            src_ref=src, dst_ref=dst, send_sem=r_sent.at[1 - main], recv_sem=r_recv.at[1 - main],
+            device_id=peer, device_id_type=MESH,
+        )
+
+    low_rows = lax.broadcasted_iota(jnp.int32, (128, 256), 0) % 8 < 4
+
+    def fold(half, block):
+        left = slice(block * 256, block * 256 + 256)
+        right = slice(1024 + block * 256, 1280 + block * 256)
+        if half == 0:
+            rows = jnp.where(low_rows, orx[:, left], pltpu.roll(orx[:, right], 4, 0))
+        else:
+            rows = jnp.where(low_rows, pltpu.roll(orx[:, left], 124, 0), orx[:, right])
+        rest_out[half, :, :, left] = rows.reshape(16, 8, 256).astype(bf16)
 
     with jax.named_scope("s_back0"):
         for k in range(15):
-            back(k).start()
+            back(k, 1).start()
+        for block in range(4):
+            fold(0, block)
+        for k in range(15):
+            back(k, 0).start()
         bm[me, 0:32] = rm[me, 0:32]
+        rest_in[0, me] = rest_out[0, me]
 
     def conv_part(q):
         at = pl.ds(pl.multiple_of(q * 512, 512), 512)
@@ -447,38 +483,48 @@
     weight0 = to_column(group * jax.nn.sigmoid(scores[1:2, :]), tokens)
     weight1 = to_column(group * jax.nn.sigmoid(-scores[1:2, :]), tokens)
 
-    def chosen(slot, half):
+    def chosen_main(slot, half):
         at = lax.broadcasted_iota(jnp.int32, (tokens, 512), 1)
         main = ((at // 32) * 64 + half * 32 + at % 32).astype(f32)
-        hits = jnp.where(main == slot, 1.0, 0.0).astype(bf16)
-        if half == 0:
-            return hits
-        rest = (lax.broadcasted_iota(jnp.int32, (tokens, 128), 1) + 1024).astype(f32)
-        return jnp.concatenate([hits, jnp.where(rest == slot, 1.0, 0.0).astype(bf16)], axis=1)
+        return jnp.where(main == slot, 1.0, 0.0).astype(bf16)
+
+    def chosen_rest(slot, half, right):
+        at = lax.broadcasted_iota(jnp.int32, (tokens, 128), 1)
+        name = 1024 + at + 4 * (half - right)
+        here = (at % 8 >= 4) == (right > 0)
+        return jnp.where(here & (name.astype(f32) == slot), 1.0, 0.0).astype(bf16)
+
+    def rest_rows(half, at):
+        return rest_in[half, :, :, at].astype(f32).reshape(128, 512).astype(bf16)
+
+    def weighted(pick0, pick1, rows):
+        return weight0 * jnp.dot(pick0, rows, preferred_element_type=f32) + weight1 * jnp.dot(
+            pick1, rows, preferred_element_type=f32
+        )
 
     def combine0(q):
         at = pl.ds(pl.multiple_of(q * 512, 512), 512)
         kept = pl.ds(pl.multiple_of(q % 2 * 512, 512), 512)
-        rows = bm[:, 0:32, at].reshape(512, 512)
-        pick0, pick1 = chosen(slot0_c, 0), chosen(slot1_c, 0)
-        hidden[q // 2, :, kept] = weight0 * jnp.dot(
-            pick0, rows, preferred_element_type=f32
-        ) + weight1 * jnp.dot(pick1, rows, preferred_element_type=f32)
+        rows = jnp.concatenate([bm[:, 0:32, at].reshape(512, 512), rest_rows(0, kept)], axis=0)
+        picks = [
+            jnp.concatenate([chosen_main(slot, 0), chosen_rest(slot, 0, q // 2)], axis=1)
+            for slot in (slot0_c, slot1_c)
+        ]
+        hidden[q // 2, :, kept] = weighted(picks[0], picks[1], rows)
 
     def phase1(p, carry):
         step(p)
 
         @pl.when(p == MIDDLE + 2)
         def _():
+            arrived(cw.at[pl.ds(0, 3), pl.ds(0, 128)], cw_sem.at[1])
             for k in (1, 3, 2):
-                cw_copy(k).wait_recv()
                 cs_copy(k).start()
 
         @pl.when(p == MIDDLE + 6)
         def _():
-            for k in (1, 3, 2):
-                act_copy(k).wait_recv()
-                cs_copy(k).wait_recv()
+            arrived(acts.at[pl.ds(0, 3)], act_sem.at[1])
+            arrived(cw.at[pl.ds(0, 3), pl.ds(0, 128)], cs_sem.at[1])
 
         @pl.when((p >= MIDDLE + 9) & (p < MIDDLE + 13))
         def _():
@@ -496,8 +542,8 @@
 
         @pl.when(ready == 35)
         def _():
-            for k in range(15):
-                back(k).wait_recv()
+            arrived(bm.at[pl.ds(0, 15), pl.ds(0, 32)], r_recv.at[0])
+            arrived(rest_in.at[0, pl.ds(0, 15)], r_recv.at[1])
 
         @pl.when((ready >= 35) & (ready % 2 == 1) & (ready < 43))
         def _():
@@ -505,76 +551,82 @@
 
         return carry
 
-    def quarter(k, q, main):
-        block, peer = block_at(k, -1)
-        at = pl.ds(q * 512, 512)
+    def column(k, block, main):
+        source, peer = block_at(k, -1)
+        at = pl.ds((block if main else block - 4) * 256, 256)
         if main:
-            src, dst = rm.at[block, pl.ds(32, 32), at], bm.at[me, pl.ds(32, 32), at]
+            src, dst = rm.at[source, pl.ds(32, 32), at], bm.at[me, pl.ds(32, 32), at]
         else:
-            src, dst = rr.at[block, :, at], br.at[me, :, at]
-        return pltpu.make_async_remote_copy(
-            src_ref=src, dst_ref=dst, send_sem=q_sent.at[q, 1 - main, k],
-            recv_sem=q_recv.at[q, 1 - main, k], device_id=peer, device_id_type=MESH,
+            src, dst = rest_out.at[1, source, :, at], rest_in.at[1, me, :, at]
+        return pltpu.make_async_remote_copy(
+            src_ref=src, dst_ref=dst, send_sem=q_sent.at[1 - main],
+            recv_sem=q_recv.at[block + 4 * (1 - main)], device_id=peer, device_id_type=MESH,
         )
 
     with jax.named_scope("s_phase1"):
+
         def tail(p, carry):
             phase1(p, carry)
-            for q in range(4):
-
-                @pl.when(p == LAST - 13 + 4 * q)
-                def _(q=q):
-                    at = slice(q * 512, q * 512 + 512)
-                    rr[:, :, at] = orx[:, at].reshape(16, 8, 512).astype(bf16)
-                    for main in (1, 0):
+            for block in range(8):
+
+                @pl.when(p == LAST - 15 + 2 * block)
+                def _(block=block):
+                    at = slice(block * 256, block * 256 + 256)
+                    for k in range(15):
+                        column(k, block, 1).start()
+                    bm[me, 32:64, at] = rm[me, 32:64, at]
+                    if block >= 4:
+                        fold(1, block - 4)
                         for k in range(15):
-                            quarter(k, q, main).start()
-                    bm[me, 32:64, at] = rm[me, 32:64, at]
-                    br[me, :, at] = rr[me, :, at]
+                            column(k, block, 0).start()
+                        at = slice(block * 256 - 1024, block * 256 - 768)
+                        rest_in[1, me, :, at] = rest_out[1, me, :, at]
 
             return carry
 
         lax.fori_loop(MIDDLE, LAST, tail, 0)
 
     with jax.named_scope("s_combine1"):
-        pick0b, pick1b = chosen(slot0_c, 1), chosen(slot1_c, 1)
+        pick0, pick1 = chosen_main(slot0_c, 1), chosen_main(slot1_c, 1)
         for q in range(4):
-            for main in (1, 0):
-                for k in range(15):
-                    quarter(k, q, main).wait_recv()
+            for block in (2 * q, 2 * q + 1):
+                at = slice(block * 256, block * 256 + 256)
+                arrived(bm.at[pl.ds(0, 15), pl.ds(32, 32), pl.ds(block * 256, 256)], q_recv.at[block])
             at = slice(q * 512, q * 512 + 512)
-            rest = br[:, :, at].astype(f32).reshape(128, 512).astype(bf16)
-            rows = jnp.concatenate([bm[:, 32:64, at].reshape(512, 512), rest], axis=0)
-            total = hidden[q // 2, :, q % 2 * 512 : q % 2 * 512 + 512] + (
-                weight0 * jnp.dot(pick0b, rows, preferred_element_type=f32)
-                + weight1 * jnp.dot(pick1b, rows, preferred_element_type=f32)
-            )
-            out[:, at] = total.astype(bf16)
+            kept = slice(q % 2 * 512, q % 2 * 512 + 512)
+            hidden[q // 2, :, kept] += weighted(pick0, pick1, bm[:, 32:64, at].reshape(512, 512))
+        picks = [[chosen_rest(slot, 1, right) for slot in (slot0_c, slot1_c)] for right in range(2)]
+        for part in range(2):
+            for block in (2 * part, 2 * part + 1):
+                arrived(rest_in.at[1, pl.ds(0, 15), :, pl.ds(block * 256, 256)], q_recv.at[8 + block])
+            kept = slice(part * 512, part * 512 + 512)
+            rows = rest_rows(1, kept)
+            for right in range(2):
+                total = hidden[right, :, kept] + weighted(picks[right][0], picks[right][1], rows)
+                out[:, right * 1024 + part * 512 : right * 1024 + part * 512 + 512] = total.astype(bf16)
 
     with jax.named_scope("s_sent"):
         halo.wait_send()
-        for k in (1, 3, 2):
-            stat_copy(k).wait_send()
-            act_copy(k).wait_send()
-            cw_copy(k).wait_send()
-            cs_copy(k).wait_send()
-        for k in range(15):
-            for part in range(3):
-                dispatch(k, part).wait_send()
-            back(k).wait_send()
-            for q in range(4):
-                for main in (1, 0):
-                    quarter(k, q, main).wait_send()
-
-        def sent(n, carry):
-            @pl.when((dist < 3) | (n < CHUNKS))
-            def _():
-                ring_copy(n, avail).wait_send()
-
-            sib_copy(hs, n, share).wait_send()
-            return carry
-
-        lax.fori_loop(0, TOTAL, sent, 0)
+        arrived(stat.at[pl.ds(0, 3)], stat_sem.at[0])
+        arrived(acts.at[pl.ds(0, 3)], act_sem.at[0])
+        arrived(cw.at[pl.ds(0, 3), pl.ds(0, 128)], cw_sem.at[0])
+        arrived(cw.at[pl.ds(0, 3), pl.ds(0, 128)], cs_sem.at[0])
+        arrived(sm.at[pl.ds(0, 15)], d_sent.at[0])
+        arrived(sr.at[pl.ds(0, 15)], d_sent.at[1])
+        arrived(bm.at[pl.ds(0, 15), pl.ds(0, 32)], r_sent.at[0])
+        arrived(rest_in.at[0, pl.ds(0, 15)], r_sent.at[1])
+        arrived(bm.at[pl.ds(0, 15), pl.ds(32, 32)], q_sent.at[0])
+        arrived(rest_in.at[1, pl.ds(0, 15)], q_sent.at[1])
+
+        @pl.when(dist < 3)
+        def _():
+            arrived(w.at[0], ring_sent)
+
+        @pl.when(dist == 3)
+        def _():
+            arrived(w.at[0, 0], ring_sent)
+
+        arrived(w.at[0], sib_sent)
 
 
 def on_device(
@@ -601,10 +653,10 @@
     return pl.pallas_call(
         kernel,
         out_shape=(
-            jax.ShapeDtypeStruct((span // NY, width), bf16),
-            jax.ShapeDtypeStruct((rows, width), bf16),
+            pltpu.VMEM((span // NY, width), bf16),
+            pltpu.VMEM((rows, width), bf16),
         ),
-        in_specs=[hbm, hbm, hbm, vmem, vmem, hbm, hbm, vmem, vmem, vmem, hbm, hbm, hbm],
+        in_specs=[hbm] * 13,
         out_specs=(vmem, vmem),
         scratch_shapes=[
             pltpu.VMEM((2, 2, CHUNKS * PIECE, 256), bf16),
@@ -614,7 +666,8 @@
             pltpu.VMEM((16, 64, width), bf16),
             pltpu.VMEM((16, 8, width), bf16),
             pltpu.VMEM((16, 64, width), bf16),
-            pltpu.VMEM((16, 8, width), bf16),
+            pltpu.VMEM((2, 16, 8, width // 2), bf16),
+            pltpu.VMEM((2, 16, 8, width // 2), bf16),
             pltpu.VMEM((2, 384, 1024), f32),
             pltpu.VMEM((2, 384, 512), bf16),
             pltpu.VMEM((128, width), bf16),
@@ -622,6 +675,11 @@
             pltpu.VMEM((span, channels), bf16),
             pltpu.VMEM((span, channels), bf16),
             pltpu.VMEM((KERNEL, channels), f32),
+            pltpu.VMEM((1, channels), f32),
+            pltpu.VMEM((1, channels), f32),
+            pltpu.VMEM((1, width), f32),
+            pltpu.VMEM((2, rows), jnp.int32),
+            pltpu.VMEM((2, rows), f32),
             pltpu.VMEM((HALO + span, channels), f32),
             pltpu.VMEM((NY, span // NY, channels), bf16),
             pltpu.VMEM((NY, channels, width), bf16),
@@ -630,30 +688,26 @@
             pltpu.VMEM((HALO, channels), bf16),
             pltpu.VMEM((NY, 16, 128), f32),
             pltpu.VMEM((16, 128), f32),
-            dma((5,)),
+            dma((10,)),
+            dma((6,)),
             dma((TOTAL,)),
-            dma((TOTAL,)),
-            dma((TOTAL,)),
+            dma((24,)),
             dma,
             dma,
-            dma((3, 15)),
-            dma((3, 15)),
-            dma((15,)),
-            dma((15,)),
-            dma((4, 2, 15)),
-            dma((4, 2, 15)),
-            dma((2,)),
-            dma((4,)),
-            dma((4,)),
-            dma((4,)),
-            dma((4,)),
-            dma((4,)),
-            dma((4,)),
-            dma((4,)),
-            dma((4,)),
+            dma((2,)),
+            dma((3,)),
+            dma((2,)),
+            dma((2,)),
+            dma((2,)),
+            dma((12,)),
+            dma((2,)),
+            dma((2,)),
+            dma((2,)),
+            dma((2,)),
+            dma((2,)),
         ],
         compiler_params=pltpu.CompilerParams(
-            collective_id=0, has_side_effects=True, vmem_limit_bytes=67_000_000
+            collective_id=0, has_side_effects=True, vmem_limit_bytes=62_000_000
         ),
         name="both",
     )(

time: 191 us -> 180 us (0.942); the launches traced: 190 us -> 177 us
  Pallas kernels: 185 us -> 174 us
    pallas_call x1, Pallas kernels: 185 us -> 174 us  [on_device(): pl.pallas_call(kernel, out_shape=(pltpu.VMEM((span // NY, width), bf16),...]
where the time goes in v4:
time: 180 us; the launch traced here: 177 us
  Pallas kernels  174 us (97%)
  local copies, waits for them, and re-layouts  2.11 us (1%)
    pallas_call x1, Pallas kernels, on_device(): pl.pallas_call(kernel, out_shape=(pltpu.VMEM((span // NY, width), bf16),...  174 us

profile of v4, /device:TPU:2, one launch (start us, length us, event | category | flops | bytes accessed | tf_op | source)
XLA Modules:
  0.0 176.6 jit_solution(1510215277776907947)
XLA Ops:
  0.6 173.8 %both.1 = (bf16[256,2048]{1,0:T(8,128)(2,1)S(1)}, bf16[384,2048]{1,0:T(8,128)(2,1)S(1)}) custom-call(bf16[1024,256]{1,0:T(8,128)(2,1)} %value_hbm.1, bf16[1024,256]{1,0:T(8,128)(2,1)} %gate_hbm.1, f32[31,1024]{1,0:T(8,128)} %taps_hbm.1, f32[1,1024]{1,0:T(1,128)} %bitcast.6, f32[1,1024]{1,0:T(1,128)} %bitcast.7, bf16[256,2048]{1,0:T(8,128)(2,1)} %cw_hbm.1, ...), custom_call_target="tpu_custom_call" | custom-call | tf_op jit(solution)/shard_map/both/pallas_call | solution.py:653
  174.4 1.0 copy.17
  175.4 1.1 copy.18

commit v5 on v4

--- a/solution.py
+++ b/solution.py
@@ -372,21 +372,18 @@
         e_low = jnp.where((dist == 0) & (c == 1), 1 - half, half)
         return jnp.where(s == 0, h_low, 1 - h_low), jnp.where(s == 0, e_low, 1 - e_low)
 
-    def shared(half, low, count):
-        others = jnp.where(dist == 0, 1 - c, jnp.where(c == 0, 1 - half, half))
-
-        @pl.when((dist > 0) | (half == 0))
-        def _():
-            arrived(w.at[hs, 0, pl.ds(0, count * PIECE)], share_of(others * CHUNKS + low))
+    def shared(half, s, low, count):
+        e = of_half(half, s)[1]
+
+        @pl.when(jnp.where(dist > 0, s != c, (s == 1) & (half == 0)))
+        def _():
+            arrived(w.at[hs, 0, pl.ds(0, count * PIECE)], share_of(e * CHUNKS + low))
 
     def rows_at(half, s):
         return pl.ds(pl.multiple_of(half * 32 + s * MAIN, MAIN), MAIN)
 
     def gate_up(half, block, s):
-        @pl.when(s == 0)
-        def _():
-            shared(half, block * 8, 8)
-
+        shared(half, s, block * 8, 8)
         h, e = of_half(half, s)
         rows = jnp.concatenate([rm[:, rows_at(half, s), :].reshape(256, 2048), rx[...]], axis=0)
         weight = w[h, e, pl.ds(pl.multiple_of(block * 2048, 2048), 2048), :]
@@ -397,16 +394,15 @@
         def _():
             inner[s] = (jax.nn.silu(hidden[s, :, 0:512]) * hidden[s, :, 512:1024]).astype(bf16)
 
-    def down(half, block):
-        shared(half, 32 + block * 2, 2)
+    def down(half, block, s):
+        shared(half, s, 32 + block * 2, 2)
         at = pl.ds(pl.multiple_of(block * 256, 256), 256)
-        for s in range(2):
-            h, e = of_half(half, s)
-            weight = w[h, e, pl.ds(pl.multiple_of(8192 + block * 512, 512), 512), :]
-            rows = jnp.dot(inner[s], weight, preferred_element_type=f32)
-            rm[:, rows_at(half, s), at] = rows[:256].astype(bf16).reshape(16, MAIN, 256)
-            here = order_in_rest == half * 2 + s
-            orx[:, at] = jnp.where(here, rows[256:], orx[:, at])
+        h, e = of_half(half, s)
+        weight = w[h, e, pl.ds(pl.multiple_of(8192 + block * 512, 512), 512), :]
+        rows = jnp.dot(inner[s], weight, preferred_element_type=f32)
+        rm[:, rows_at(half, s), at] = rows[:256].astype(bf16).reshape(16, MAIN, 256)
+        here = order_in_rest == half * 2 + s
+        orx[:, at] = jnp.where(here, rows[256:], orx[:, at])
 
     def activate(b):
         rows = pl.ds(pl.multiple_of(b * 128, 128), 128)
@@ -431,7 +427,8 @@
 
         @pl.when(p >= START + 8)
         def _():
-            down(0, p - START - 8)
+            for s in range(2):
+                down(0, p - START - 8, s)
 
         return carry
 
@@ -512,33 +509,79 @@
         ]
         hidden[q // 2, :, kept] = weighted(picks[0], picks[1], rows)
 
+    def column(k, q, s):
+        source, peer = block_at(k, -1)
+        at = pl.ds(pl.multiple_of(q * 512, 512), 512)
+        rows = pl.ds(32 + s * MAIN, MAIN)
+        return pltpu.make_async_remote_copy(
+            src_ref=rm.at[source, rows, at], dst_ref=bm.at[me, rows, at], send_sem=q_sent.at[0],
+            recv_sem=q_recv.at[s * 4 + q], device_id=peer, device_id_type=MESH,
+        )
+
+    def rest_column(k, q):
+        source, peer = block_at(k, -1)
+        at = pl.ds(q * 512, 512)
+        return pltpu.make_async_remote_copy(
+            src_ref=rest_out.at[1, source, :, at], dst_ref=rest_in.at[1, me, :, at],
+            send_sem=q_sent.at[1], recv_sem=q_recv.at[8 + q], device_id=peer, device_id_type=MESH,
+        )
+
+    def leave(q, s):
+        at = pl.ds(pl.multiple_of(q * 512, 512), 512)
+        rows = pl.ds(32 + s * MAIN, MAIN)
+        for k in range(15):
+            column(k, q, s).start()
+        bm[me, rows, at] = rm[me, rows, at]
+
+    def rest_leave(q):
+        fold(1, 2 * q)
+        fold(1, 2 * q + 1)
+        for k in range(15):
+            rest_column(k, q).start()
+        at = slice(q * 512, q * 512 + 512)
+        rest_in[1, me, :, at] = rest_out[1, me, :, at]
+
     def phase1(p, carry):
         step(p)
 
-        @pl.when(p == MIDDLE + 2)
+        @pl.when(p == MIDDLE + 14)
         def _():
             arrived(cw.at[pl.ds(0, 3), pl.ds(0, 128)], cw_sem.at[1])
             for k in (1, 3, 2):
                 cs_copy(k).start()
 
-        @pl.when(p == MIDDLE + 6)
+        @pl.when(p == MIDDLE + 20)
         def _():
             arrived(acts.at[pl.ds(0, 3)], act_sem.at[1])
             arrived(cw.at[pl.ds(0, 3), pl.ds(0, 128)], cs_sem.at[1])
 
-        @pl.when((p >= MIDDLE + 9) & (p < MIDDLE + 13))
-        def _():
-            conv_part(p - MIDDLE - 9)
+        @pl.when((p >= MIDDLE + 20) & (p < MIDDLE + 24))
+        def _():
+            conv_part(p - MIDDLE - 20)
 
         ready = p - FAR - CHUNKS + 1
 
-        @pl.when((ready >= 8) & (ready < 34) & (ready % 8 < 2))
-        def _():
-            gate_up(1, ready // 8 - 1, ready % 8)
-
-        @pl.when((ready >= 34) & (ready % 2 == 0))
-        def _():
-            down(1, (ready - 34) // 2)
+        for s in range(2):
+            handed = jnp.where(c == s, HOP * dist, HOP * (4 - dist) + 3)
+            lag = jnp.where(dist == 0, 0, handed)
+
+            def pieces(p, lag=lag):
+                return jnp.minimum(2 * (p - MIDDLE), p - lag - CHUNKS + 1)
+
+            old, new = pieces(p - 1), pieces(p)
+
+            @pl.when((new >= 8) & (new < 34) & (new // 8 != old // 8))
+            def _(s=s, new=new):
+                gate_up(1, new // 8 - 1, s)
+
+            @pl.when((new >= 34) & (new < 50) & (new // 2 != old // 2))
+            def _(s=s, new=new):
+                block = (new - 34) // 2
+                down(1, block, s)
+
+                @pl.when(block % 2 == 1)
+                def _():
+                    leave(block // 2, s)
 
         @pl.when(ready == 35)
         def _():
@@ -549,56 +592,31 @@
         def _():
             combine0((ready - 35) // 2)
 
+        for q in range(2):
+
+            @pl.when(p == LAST - 5 + 4 * q)
+            def _(q=q):
+                rest_leave(q)
+
         return carry
 
-    def column(k, block, main):
-        source, peer = block_at(k, -1)
-        at = pl.ds((block if main else block - 4) * 256, 256)
-        if main:
-            src, dst = rm.at[source, pl.ds(32, 32), at], bm.at[me, pl.ds(32, 32), at]
-        else:
-            src, dst = rest_out.at[1, source, :, at], rest_in.at[1, me, :, at]
-        return pltpu.make_async_remote_copy(
-            src_ref=src, dst_ref=dst, send_sem=q_sent.at[1 - main],
-            recv_sem=q_recv.at[block + 4 * (1 - main)], device_id=peer, device_id_type=MESH,
-        )
-
     with jax.named_scope("s_phase1"):
-
-        def tail(p, carry):
-            phase1(p, carry)
-            for block in range(8):
-
-                @pl.when(p == LAST - 15 + 2 * block)
-                def _(block=block):
-                    at = slice(block * 256, block * 256 + 256)
-                    for k in range(15):
-                        column(k, block, 1).start()
-                    bm[me, 32:64, at] = rm[me, 32:64, at]
-                    if block >= 4:
-                        fold(1, block - 4)
-                        for k in range(15):
-                            column(k, block, 0).start()
-                        at = slice(block * 256 - 1024, block * 256 - 768)
-                        rest_in[1, me, :, at] = rest_out[1, me, :, at]
-
-            return carry
-
-        lax.fori_loop(MIDDLE, LAST, tail, 0)
+        lax.fori_loop(MIDDLE, LAST, phase1, 0)
 
     with jax.named_scope("s_combine1"):
         pick0, pick1 = chosen_main(slot0_c, 1), chosen_main(slot1_c, 1)
         for q in range(4):
-            for block in (2 * q, 2 * q + 1):
-                at = slice(block * 256, block * 256 + 256)
-                arrived(bm.at[pl.ds(0, 15), pl.ds(32, 32), pl.ds(block * 256, 256)], q_recv.at[block])
+            for s in range(2):
+                arrived(
+                    bm.at[pl.ds(0, 15), pl.ds(32 + s * MAIN, MAIN), pl.ds(q * 512, 512)],
+                    q_recv.at[s * 4 + q],
+                )
             at = slice(q * 512, q * 512 + 512)
             kept = slice(q % 2 * 512, q % 2 * 512 + 512)
             hidden[q // 2, :, kept] += weighted(pick0, pick1, bm[:, 32:64, at].reshape(512, 512))
         picks = [[chosen_rest(slot, 1, right) for slot in (slot0_c, slot1_c)] for right in range(2)]
         for part in range(2):
-            for block in (2 * part, 2 * part + 1):
-                arrived(rest_in.at[1, pl.ds(0, 15), :, pl.ds(block * 256, 256)], q_recv.at[8 + block])
+            arrived(rest_in.at[1, pl.ds(0, 15), :, pl.ds(part * 512, 512)], q_recv.at[8 + part])
             kept = slice(part * 512, part * 512 + 512)
             rows = rest_rows(1, kept)
             for right in range(2):
@@ -699,7 +717,7 @@
             dma((2,)),
             dma((2,)),
             dma((2,)),
-            dma((12,)),
+            dma((10,)),
             dma((2,)),
             dma((2,)),
             dma((2,)),

time: 180 us -> 172 us (0.956); the launches traced: 177 us -> 172 us
  Pallas kernels: 174 us -> 169 us
    pallas_call x1, Pallas kernels: 174 us -> 169 us  [on_device(): pl.pallas_call(kernel, out_shape=(pltpu.VMEM((span // NY, width), bf16),...]
where the time goes in v5:
time: 172 us
  Pallas kernels  169 us (98%)
  local copies, waits for them, and re-layouts  2.11 us (1%)
    pallas_call x1, Pallas kernels, on_device(): pl.pallas_call(kernel, out_shape=(pltpu.VMEM((span // NY, width), bf16),...  169 us

profile of v5, /device:TPU:2, one launch (start us, length us, event | category | flops | bytes accessed | tf_op | source)
XLA Modules:
  0.0 171.9 jit_solution(2077193406402087444)
XLA Ops:
  0.6 169.1 %both.1 = (bf16[256,2048]{1,0:T(8,128)(2,1)S(1)}, bf16[384,2048]{1,0:T(8,128)(2,1)S(1)}) custom-call(bf16[1024,256]{1,0:T(8,128)(2,1)} %value_hbm.1, bf16[1024,256]{1,0:T(8,128)(2,1)} %gate_hbm.1, f32[31,1024]{1,0:T(8,128)} %taps_hbm.1, f32[1,1024]{1,0:T(1,128)} %bitcast.6, f32[1,1024]{1,0:T(1,128)} %bitcast.7, bf16[256,2048]{1,0:T(8,128)(2,1)} %cw_hbm.1, ...), custom_call_target="tpu_custom_call" | custom-call | tf_op jit(solution)/shard_map/both/pallas_call | solution.py:671
  169.7 1.0 copy.17
  170.7 1.1 copy.18

commit v6 on v5

--- a/solution.py
+++ b/solution.py
@@ -15,16 +15,19 @@
 PIECE = 256
 CHUNKS = 48
 TOTAL = 2 * CHUNKS
-HOP = 4
-FAR = 3 * HOP + 3
-OUTER = 4 * HOP + 2
-START = 50
+HOP = 2
+AHEAD = 4
+SHARE = 4
+OUTER = 12
+START = 48
 MIDDLE = START + 16
-LAST = TOTAL + FAR
+LAST = TOTAL + 3 * HOP + SHARE
 OFFSETS = [
     (1, 0), (3, 0), (0, 1), (0, 3), (1, 1), (3, 3), (1, 3), (3, 1),
     (2, 0), (0, 2), (2, 2), (1, 2), (3, 2), (2, 1), (2, 3),
 ]
+
+TAIL_ORDER = tuple(reversed(range(15)))
 
 
 def slot_of(expert, rank, z, c):
@@ -62,7 +65,7 @@
     value_hbm, gate_hbm, taps_hbm, gain_c_hbm, shift_c_hbm, cw_hbm,
     x_hbm, gain_hbm, experts_hbm, scores_hbm, wg_hbm, wu_hbm, wd_hbm,
     conv_out, out,
-    w, xn, sm, sr, rm, sx, bm, rest_out, rest_in, hidden, inner, rx, orx,
+    w, xn, sm, sr, rm, sx, bm, rest_out, rest_in, hidden, sums, inner, rx, orx,
     val, gat, taps, gain_c, shift_c, gain, experts, scores,
     pad, acts, cw, window, halo_out, halo_in, stat, stats,
     load, native, avail, share, ring_sent, sib_sent,
@@ -171,7 +174,7 @@
             sib_copy(hs, i, avail.at[i]).start()
 
     def step(p):
-        n = p - HOP * dist
+        n = p + jnp.where(dist == 0, AHEAD, -HOP * dist)
         m = p - OUTER
 
         @pl.when((n >= 0) & (n < TOTAL))
@@ -232,24 +235,62 @@
     with jax.named_scope("s_barrier"):
         pl.semaphore_wait(barrier, len(peers))
     halo.start()
+
+    @pl.when(dist == 0)
+    def _():
+        for n in range(AHEAD):
+            own(n)
+
     step(0)
 
     def picked(base, count):
         at = (lax.broadcasted_iota(jnp.int32, (count, tokens), 0) + base).astype(f32)
         return jnp.where((at == slot0) | (at == slot1), 1.0, 0.0).astype(bf16)
 
+    def dispatch(xx, yy, part):
+        block = xx * NY + yy
+        if part < 2:
+            src, dst = sm.at[block, pl.ds(part * 32, 32)], rm.at[me, pl.ds(part * 32, 32)]
+        else:
+            src, dst = sr.at[block], sx.at[me]
+        return pltpu.make_async_remote_copy(
+            src_ref=src, dst_ref=dst, send_sem=d_sent.at[part // 2], recv_sem=d_recv.at[part],
+            device_id=(device(z, xx, c), yy), device_id_type=MESH,
+        )
+
+    def column_of(g):
+        return (x + jnp.where(g == 0, 1, jnp.where(g == 1, 3, jnp.where(g == 2, 2, 0)))) % NX
+
+    def send_group(g):
+        xx = column_of(g)
+        for part in range(2):
+            for dy in (1, 3, 2, 0):
+                copy = dispatch(xx, (y + dy) % NY, part)
+                if dy > 0:
+                    copy.start()
+                else:
+
+                    @pl.when(g < 3)
+                    def _(copy=copy):
+                        copy.start()
+
     def gather(g, carry):
-        choose = picked(g * 256, 256)
+        xx = column_of(g)
+        choose = picked(xx * 256, 256)
 
         def cols(q, carry):
             at = pl.ds(pl.multiple_of(q * 512, 512), 512)
             rows = jnp.dot(choose, xn[:, at], preferred_element_type=f32).astype(bf16)
-            sm[pl.ds(g * 4, 4), :, at] = rows.reshape(4, 64, 512)
+            sm[pl.ds(xx * 4, 4), :, at] = rows.reshape(4, 64, 512)
             return carry
 
         lax.fori_loop(0, 4, cols, 0)
-
         step(1 + g)
+
+        @pl.when(g > 0)
+        def _():
+            send_group(g - 1)
+
         return carry
 
     with jax.named_scope("s_gather"):
@@ -269,21 +310,10 @@
         xx, yy = (x + sign * dx + NX) % NX, (y + sign * dy + NY) % NY
         return xx * NY + yy, (device(z, xx, c), yy)
 
-    def dispatch(k, part):
-        block, peer = block_at(k, 1)
-        if part < 2:
-            src, dst = sm.at[block, pl.ds(part * 32, 32)], rm.at[me, pl.ds(part * 32, 32)]
-        else:
-            src, dst = sr.at[block], sx.at[me]
-        return pltpu.make_async_remote_copy(
-            src_ref=src, dst_ref=dst, send_sem=d_sent.at[part // 2], recv_sem=d_recv.at[part],
-            device_id=peer, device_id_type=MESH,
-        )
-
     with jax.named_scope("s_dispatch"):
-        for part in range(3):
-            for k in range(15):
-                dispatch(k, part).start()
+        send_group(3)
+        for dx, dy in OFFSETS:
+            dispatch((x + dx) % NX, (y + dy) % NY, 2).start()
         rm[me] = sm[me]
         sx[me] = sr[me]
 
@@ -411,13 +441,10 @@
         normed = (pad[rows, :] - center) * lax.rsqrt(spread + 1e-05) * gain_c[...] + shift_c[...]
         val[rows, :] = jax.nn.silu(normed).astype(bf16)
 
-    def phase0(p, carry):
-        step(p)
-
+    def phase0(p):
         @pl.when(p < START + 8)
         def _():
             activate(p - START)
-            gate_up(0, (p - START) // 2, (p - START) % 2)
 
         @pl.when(p == START + 8)
         def _():
@@ -425,15 +452,16 @@
                 act_copy(k).start()
             acts[y] = val[my_cols, :]
 
-        @pl.when(p >= START + 8)
+        q = p - START
+
+        @pl.when((q >= 0) & (q < 8))
+        def _():
+            gate_up(0, q // 2, q % 2)
+
+        @pl.when((q >= 8) & (q < 16))
         def _():
             for s in range(2):
-                down(0, p - START - 8, s)
-
-        return carry
-
-    with jax.named_scope("s_phase0"):
-        lax.fori_loop(START, MIDDLE, phase0, 0)
+                down(0, q - 8, s)
 
     def back(k, main):
         block, peer = block_at(k, -1)
@@ -457,7 +485,7 @@
             rows = jnp.where(low_rows, pltpu.roll(orx[:, left], 124, 0), orx[:, right])
         rest_out[half, :, :, left] = rows.reshape(16, 8, 256).astype(bf16)
 
-    with jax.named_scope("s_back0"):
+    def first_leave():
         for k in range(15):
             back(k, 1).start()
         for block in range(4):
@@ -492,78 +520,82 @@
         return jnp.where(here & (name.astype(f32) == slot), 1.0, 0.0).astype(bf16)
 
     def rest_rows(half, at):
-        return rest_in[half, :, :, at].astype(f32).reshape(128, 512).astype(bf16)
+        return rest_in[half, :, :, at].astype(f32).reshape(128, 256).astype(bf16)
 
     def weighted(pick0, pick1, rows):
         return weight0 * jnp.dot(pick0, rows, preferred_element_type=f32) + weight1 * jnp.dot(
             pick1, rows, preferred_element_type=f32
         )
 
-    def combine0(q):
-        at = pl.ds(pl.multiple_of(q * 512, 512), 512)
-        kept = pl.ds(pl.multiple_of(q % 2 * 512, 512), 512)
-        rows = jnp.concatenate([bm[:, 0:32, at].reshape(512, 512), rest_rows(0, kept)], axis=0)
+    def combine0(block):
+        at = slice(block * 256, block * 256 + 256)
+        folded = slice(block % 4 * 256, block % 4 * 256 + 256)
+        rows = jnp.concatenate([bm[:, 0:32, at].reshape(512, 256), rest_rows(0, folded)], axis=0)
         picks = [
-            jnp.concatenate([chosen_main(slot, 0), chosen_rest(slot, 0, q // 2)], axis=1)
+            jnp.concatenate([chosen_main(slot, 0), chosen_rest(slot, 0, block // 4)], axis=1)
             for slot in (slot0_c, slot1_c)
         ]
-        hidden[q // 2, :, kept] = weighted(picks[0], picks[1], rows)
-
-    def column(k, q, s):
+        sums[:, at] = weighted(picks[0], picks[1], rows)
+
+    def column(k, block, s):
         source, peer = block_at(k, -1)
-        at = pl.ds(pl.multiple_of(q * 512, 512), 512)
+        at = pl.ds(pl.multiple_of(block * 256, 256), 256)
         rows = pl.ds(32 + s * MAIN, MAIN)
         return pltpu.make_async_remote_copy(
             src_ref=rm.at[source, rows, at], dst_ref=bm.at[me, rows, at], send_sem=q_sent.at[0],
-            recv_sem=q_recv.at[s * 4 + q], device_id=peer, device_id_type=MESH,
-        )
-
-    def rest_column(k, q):
+            recv_sem=q_recv.at[block], device_id=peer, device_id_type=MESH,
+        )
+
+    def rest_column(k, block):
         source, peer = block_at(k, -1)
-        at = pl.ds(q * 512, 512)
+        at = pl.ds(block * 256, 256)
         return pltpu.make_async_remote_copy(
             src_ref=rest_out.at[1, source, :, at], dst_ref=rest_in.at[1, me, :, at],
-            send_sem=q_sent.at[1], recv_sem=q_recv.at[8 + q], device_id=peer, device_id_type=MESH,
-        )
-
-    def leave(q, s):
-        at = pl.ds(pl.multiple_of(q * 512, 512), 512)
+            send_sem=q_sent.at[1], recv_sem=q_recv.at[8 + block], device_id=peer,
+            device_id_type=MESH,
+        )
+
+    def leave(block, s):
+        at = pl.ds(pl.multiple_of(block * 256, 256), 256)
         rows = pl.ds(32 + s * MAIN, MAIN)
-        for k in range(15):
-            column(k, q, s).start()
+        for k in TAIL_ORDER:
+            column(k, block, s).start()
         bm[me, rows, at] = rm[me, rows, at]
 
-    def rest_leave(q):
-        fold(1, 2 * q)
-        fold(1, 2 * q + 1)
-        for k in range(15):
-            rest_column(k, q).start()
-        at = slice(q * 512, q * 512 + 512)
+    def rest_leave(block):
+        fold(1, block)
+        for k in TAIL_ORDER:
+            rest_column(k, block).start()
+        at = slice(block * 256, block * 256 + 256)
         rest_in[1, me, :, at] = rest_out[1, me, :, at]
 
-    def phase1(p, carry):
+    def phases(p, carry):
         step(p)
-
-        @pl.when(p == MIDDLE + 14)
+        phase0(p)
+
+        @pl.when(p == MIDDLE)
+        def _():
+            first_leave()
+
+        @pl.when(p == MIDDLE + 10)
         def _():
             arrived(cw.at[pl.ds(0, 3), pl.ds(0, 128)], cw_sem.at[1])
             for k in (1, 3, 2):
                 cs_copy(k).start()
 
-        @pl.when(p == MIDDLE + 20)
+        @pl.when(p == MIDDLE + 18)
         def _():
             arrived(acts.at[pl.ds(0, 3)], act_sem.at[1])
             arrived(cw.at[pl.ds(0, 3), pl.ds(0, 128)], cs_sem.at[1])
 
-        @pl.when((p >= MIDDLE + 20) & (p < MIDDLE + 24))
-        def _():
-            conv_part(p - MIDDLE - 20)
-
-        ready = p - FAR - CHUNKS + 1
-
+        @pl.when((p >= MIDDLE + 18) & (p < MIDDLE + 22))
+        def _():
+            conv_part(p - MIDDLE - 18)
+
+        there = []
         for s in range(2):
-            handed = jnp.where(c == s, HOP * dist, HOP * (4 - dist) + 3)
-            lag = jnp.where(dist == 0, 0, handed)
+            handed = jnp.where(c == s, HOP * dist, HOP * (4 - dist) + SHARE)
+            lag = jnp.where(dist == 0, -AHEAD, handed)
 
             def pieces(p, lag=lag):
                 return jnp.minimum(2 * (p - MIDDLE), p - lag - CHUNKS + 1)
@@ -578,50 +610,44 @@
             def _(s=s, new=new):
                 block = (new - 34) // 2
                 down(1, block, s)
-
-                @pl.when(block % 2 == 1)
-                def _():
-                    leave(block // 2, s)
-
-        @pl.when(ready == 35)
-        def _():
-            arrived(bm.at[pl.ds(0, 15), pl.ds(0, 32)], r_recv.at[0])
-            arrived(rest_in.at[0, pl.ds(0, 15)], r_recv.at[1])
-
-        @pl.when((ready >= 35) & (ready % 2 == 1) & (ready < 43))
-        def _():
-            combine0((ready - 35) // 2)
-
-        for q in range(2):
-
-            @pl.when(p == LAST - 5 + 4 * q)
-            def _(q=q):
-                rest_leave(q)
+                leave(block, s)
+
+            there.append((old, new))
+
+        old, new = [jnp.minimum(there[0][i], there[1][i]) for i in range(2)]
+        for block in range(4):
+            due = 42 + 2 * block
+
+            @pl.when((old < due) & (new >= due))
+            def _(block=block):
+                rest_leave(block)
 
         return carry
 
     with jax.named_scope("s_phase1"):
-        lax.fori_loop(MIDDLE, LAST, phase1, 0)
+        lax.fori_loop(START, LAST, phases, 0)
+
+    with jax.named_scope("s_combine0"):
+        arrived(bm.at[pl.ds(0, 15), pl.ds(0, 32)], r_recv.at[0])
+        arrived(rest_in.at[0, pl.ds(0, 15)], r_recv.at[1])
+        for block in range(8):
+            combine0(block)
 
     with jax.named_scope("s_combine1"):
         pick0, pick1 = chosen_main(slot0_c, 1), chosen_main(slot1_c, 1)
-        for q in range(4):
-            for s in range(2):
-                arrived(
-                    bm.at[pl.ds(0, 15), pl.ds(32 + s * MAIN, MAIN), pl.ds(q * 512, 512)],
-                    q_recv.at[s * 4 + q],
-                )
-            at = slice(q * 512, q * 512 + 512)
-            kept = slice(q % 2 * 512, q % 2 * 512 + 512)
-            hidden[q // 2, :, kept] += weighted(pick0, pick1, bm[:, 32:64, at].reshape(512, 512))
         picks = [[chosen_rest(slot, 1, right) for slot in (slot0_c, slot1_c)] for right in range(2)]
-        for part in range(2):
-            arrived(rest_in.at[1, pl.ds(0, 15), :, pl.ds(part * 512, 512)], q_recv.at[8 + part])
-            kept = slice(part * 512, part * 512 + 512)
-            rows = rest_rows(1, kept)
-            for right in range(2):
-                total = hidden[right, :, kept] + weighted(picks[right][0], picks[right][1], rows)
-                out[:, right * 1024 + part * 512 : right * 1024 + part * 512 + 512] = total.astype(bf16)
+        for block in range(8):
+            at = slice(block * 256, block * 256 + 256)
+            arrived(bm.at[pl.ds(0, 15), pl.ds(32, 32), pl.ds(block * 256, 256)], q_recv.at[block])
+            sums[:, at] += weighted(pick0, pick1, bm[:, 32:64, at].reshape(512, 256))
+            if block >= 4:
+                low = block * 256 - 1024
+                arrived(rest_in.at[1, pl.ds(0, 15), :, pl.ds(low, 256)], q_recv.at[4 + block])
+                rows = rest_rows(1, slice(low, low + 256))
+                for right in range(2):
+                    at = slice(low + right * 1024, low + right * 1024 + 256)
+                    last = weighted(picks[right][0], picks[right][1], rows)
+                    out[:, at] = (sums[:, at] + last).astype(bf16)
 
     with jax.named_scope("s_sent"):
         halo.wait_send()
@@ -645,6 +671,19 @@
             arrived(w.at[0, 0], ring_sent)
 
         arrived(w.at[0], sib_sent)
+
+
+def write_out(conv_ref, moe_ref, conv_out, moe_out, sems):
+    copies = []
+    for source, target in ((moe_ref, moe_out), (conv_ref, conv_out)):
+        for low in range(0, source.shape[0], 128):
+            rows = pl.ds(low, 128)
+            copies.append(
+                pltpu.make_async_copy(source.at[rows], target.at[rows], sems.at[len(copies)])
+            )
+            copies[-1].start()
+    for copy in copies:
+        copy.wait()
 
 
 def on_device(
@@ -668,7 +707,7 @@
     hbm = pl.BlockSpec(memory_space=pl.ANY)
     vmem = pl.BlockSpec(memory_space=pltpu.VMEM)
     dma = pltpu.SemaphoreType.DMA
-    return pl.pallas_call(
+    both = pl.pallas_call(
         kernel,
         out_shape=(
             pltpu.VMEM((span // NY, width), bf16),
@@ -687,6 +726,7 @@
             pltpu.VMEM((2, 16, 8, width // 2), bf16),
             pltpu.VMEM((2, 16, 8, width // 2), bf16),
             pltpu.VMEM((2, 384, 1024), f32),
+            pltpu.VMEM((rows, width), f32),
             pltpu.VMEM((2, 384, 512), bf16),
             pltpu.VMEM((128, width), bf16),
             pltpu.VMEM((128, width), f32),
@@ -717,7 +757,7 @@
             dma((2,)),
             dma((2,)),
             dma((2,)),
-            dma((10,)),
+            dma((12,)),
             dma((2,)),
             dma((2,)),
             dma((2,)),
@@ -725,7 +765,7 @@
             dma((2,)),
         ],
         compiler_params=pltpu.CompilerParams(
-            collective_id=0, has_side_effects=True, vmem_limit_bytes=62_000_000
+            collective_id=0, has_side_effects=True, vmem_limit_bytes=64_300_000
         ),
         name="both",
     )(
@@ -743,6 +783,15 @@
         expert_up,
         expert_down,
     )
+    outs = [jax.ShapeDtypeStruct(out.shape, out.dtype) for out in both]
+    return pl.pallas_call(
+        write_out,
+        out_shape=tuple(outs),
+        in_specs=[vmem, vmem],
+        out_specs=(hbm, hbm),
+        scratch_shapes=[dma((sum(out.shape[0] for out in outs) // 128,))],
+        name="write_out",
+    )(*(pltpu.with_memory_space_constraint(out, pltpu.VMEM) for out in both))
 
 
 def solution(mesh):

time: 172 us -> 169 us (0.983)
  local copies, waits for them, and re-layouts: 2.11 us -> 0 us
    pallas_call x1, Pallas kernels: 169 us -> 166 us  [on_device(): pl.pallas_call(kernel, out_shape=(pltpu.VMEM((span // NY, width), bf16),...]
    unnamed x2 -> x0, local copies, waits for them, and re-layouts: 2.11 us -> none
where the time goes in v6:
time: 169 us; the launch traced here: 168 us
  Pallas kernels  168 us (99%)
    pallas_call x1, Pallas kernels, on_device(): pl.pallas_call(kernel, out_shape=(pltpu.VMEM((span // NY, width), bf16),...  166 us

profile of v6, /device:TPU:2, one launch (start us, length us, event | category | flops | bytes accessed | tf_op | source)
XLA Modules:
  0.0 168.4 jit_solution(2283717764368142938)
XLA Ops:
  0.6 166.2 %both.1 = (bf16[256,2048]{1,0:T(8,128)(2,1)S(1)}, bf16[384,2048]{1,0:T(8,128)(2,1)S(1)}) custom-call(bf16[1024,256]{1,0:T(8,128)(2,1)} %value_hbm.1, bf16[1024,256]{1,0:T(8,128)(2,1)} %gate_hbm.1, f32[31,1024]{1,0:T(8,128)} %taps_hbm.1, f32[1,1024]{1,0:T(1,128)} %bitcast.6, f32[1,1024]{1,0:T(1,128)} %bitcast.7, bf16[256,2048]{1,0:T(8,128)(2,1)} %cw_hbm.1, ...), custom_call_target="tpu_custom_call" | custom-call | tf_op jit(solution)/shard_map/both/pallas_call | solution.py:710
  166.9 1.5 write_out.1

commit v7 on v6

--- a/solution.py
+++ b/solution.py
@@ -6,6 +6,7 @@
 from jax.sharding import PartitionSpec as P
 
 MESH = pl.DeviceIdType.MESH
+OUT_ROWS = 128
 NZ, NX, NC, NY = 8, 4, 2, 4
 CONV = 1024
 KERNEL = 31
@@ -69,7 +70,7 @@
     val, gat, taps, gain_c, shift_c, gain, experts, scores,
     pad, acts, cw, window, halo_out, halo_in, stat, stats,
     load, native, avail, share, ring_sent, sib_sent,
-    d_sent, d_recv, r_sent, r_recv, q_sent, q_recv,
+    sent, d_recv, r_recv, q_recv,
     halo_sem, stat_sem, act_sem, cw_sem, cs_sem,
 ):
     f32, bf16 = jnp.float32, jnp.bfloat16
@@ -92,15 +93,15 @@
 
     loads = [
         pltpu.make_async_copy(value_hbm, val, load.at[0]),
-        pltpu.make_async_copy(gate_hbm, gat, load.at[1]),
+        pltpu.make_async_copy(gate_hbm, gat, load.at[0]),
         pltpu.make_async_copy(x_hbm, xn, load.at[2]),
         pltpu.make_async_copy(taps_hbm.at[:, my_cols], taps, load.at[3]),
         pltpu.make_async_copy(cw_hbm, cw.at[y], load.at[4]),
-        pltpu.make_async_copy(gain_c_hbm.at[:, my_cols], gain_c, load.at[5]),
-        pltpu.make_async_copy(shift_c_hbm.at[:, my_cols], shift_c, load.at[6]),
-        pltpu.make_async_copy(gain_hbm, gain, load.at[7]),
-        pltpu.make_async_copy(experts_hbm, experts, load.at[8]),
-        pltpu.make_async_copy(scores_hbm, scores, load.at[9]),
+        pltpu.make_async_copy(gain_c_hbm.at[:, my_cols], gain_c, load.at[3]),
+        pltpu.make_async_copy(shift_c_hbm.at[:, my_cols], shift_c, load.at[3]),
+        pltpu.make_async_copy(gain_hbm, gain, load.at[2]),
+        pltpu.make_async_copy(experts_hbm, experts, load.at[1]),
+        pltpu.make_async_copy(scores_hbm, scores, load.at[1]),
     ]
 
     @pl.when(dist == 0)
@@ -201,7 +202,7 @@
         halo_out[...] = pad[1024 : 1024 + HALO, :].astype(bf16)
 
         halo = pltpu.make_async_remote_copy(
-            src_ref=halo_out, dst_ref=halo_in, send_sem=halo_sem.at[0], recv_sem=halo_sem.at[1],
+            src_ref=halo_out, dst_ref=halo_in, send_sem=sent, recv_sem=halo_sem,
             device_id=((ep + 1) % 64, y), device_id_type=MESH,
         )
     with jax.named_scope("s_route"):
@@ -254,7 +255,7 @@
         else:
             src, dst = sr.at[block], sx.at[me]
         return pltpu.make_async_remote_copy(
-            src_ref=src, dst_ref=dst, send_sem=d_sent.at[part // 2], recv_sem=d_recv.at[part],
+            src_ref=src, dst_ref=dst, send_sem=sent, recv_sem=d_recv.at[part],
             device_id=(device(z, xx, c), yy), device_id_type=MESH,
         )
 
@@ -320,7 +321,8 @@
     with jax.named_scope("s_filter"):
         halo.wait_recv()
         pad[0:HALO, :] = jnp.where(ep > 0, halo_in[...].astype(f32), 0.0)
-        loads[3].wait()
+        for k in (3, 5, 6):
+            loads[k].wait()
 
         def filter_block(b, carry):
             step(5 + 2 * b)
@@ -345,7 +347,7 @@
 
     def stat_copy(k):
         return pltpu.make_async_remote_copy(
-            src_ref=stat.at[y], dst_ref=stat.at[y], send_sem=stat_sem.at[0], recv_sem=stat_sem.at[1],
+            src_ref=stat.at[y], dst_ref=stat.at[y], send_sem=sent, recv_sem=stat_sem,
             device_id=near(k)[1], device_id_type=MESH,
         )
 
@@ -353,22 +355,22 @@
         yy, peer = near(k)
         return pltpu.make_async_remote_copy(
             src_ref=val.at[pl.ds(pl.multiple_of(yy * 256, 256), 256)], dst_ref=acts.at[y],
-            send_sem=act_sem.at[0], recv_sem=act_sem.at[1], device_id=peer, device_id_type=MESH,
+            send_sem=sent, recv_sem=act_sem, device_id=peer, device_id_type=MESH,
         )
 
     half = pl.ds(pl.multiple_of(c * 128, 128), 128)
 
     def cw_copy(k):
         return pltpu.make_async_remote_copy(
-            src_ref=cw.at[y, half], dst_ref=cw.at[y, half], send_sem=cw_sem.at[0],
-            recv_sem=cw_sem.at[1], device_id=near(k)[1], device_id_type=MESH,
+            src_ref=cw.at[y, half], dst_ref=cw.at[y, half], send_sem=sent,
+            recv_sem=cw_sem, device_id=near(k)[1], device_id_type=MESH,
         )
 
     def cs_copy(k):
         yy = (y + NY - k) % NY
         return pltpu.make_async_remote_copy(
-            src_ref=cw.at[yy, half], dst_ref=cw.at[yy, half], send_sem=cs_sem.at[0],
-            recv_sem=cs_sem.at[1], device_id=sibling, device_id_type=MESH,
+            src_ref=cw.at[yy, half], dst_ref=cw.at[yy, half], send_sem=sent,
+            recv_sem=cs_sem, device_id=sibling, device_id_type=MESH,
         )
 
     loads[4].wait()
@@ -391,9 +393,7 @@
         rx[...] = sx[...].astype(f32).reshape(128, 2048).astype(bf16)
 
     with jax.named_scope("s_wait_stat"):
-        arrived(stat.at[pl.ds(0, 3)], stat_sem.at[1])
-        loads[5].wait()
-        loads[6].wait()
+        arrived(stat.at[pl.ds(0, 3)], stat_sem)
         stats[...] = (stat[0] + stat[1]) + (stat[2] + stat[3])
 
     order_in_rest = (lax.broadcasted_iota(jnp.int32, (128, 256), 0) % 8) // REM
@@ -470,7 +470,7 @@
         else:
             src, dst = rest_out.at[0, block], rest_in.at[0, me]
         return pltpu.make_async_remote_copy(
-            src_ref=src, dst_ref=dst, send_sem=r_sent.at[1 - main], recv_sem=r_recv.at[1 - main],
+            src_ref=src, dst_ref=dst, send_sem=sent, recv_sem=r_recv.at[1 - main],
             device_id=peer, device_id_type=MESH,
         )
 
@@ -542,7 +542,7 @@
         at = pl.ds(pl.multiple_of(block * 256, 256), 256)
         rows = pl.ds(32 + s * MAIN, MAIN)
         return pltpu.make_async_remote_copy(
-            src_ref=rm.at[source, rows, at], dst_ref=bm.at[me, rows, at], send_sem=q_sent.at[0],
+            src_ref=rm.at[source, rows, at], dst_ref=bm.at[me, rows, at], send_sem=sent,
             recv_sem=q_recv.at[block], device_id=peer, device_id_type=MESH,
         )
 
@@ -551,7 +551,7 @@
         at = pl.ds(block * 256, 256)
         return pltpu.make_async_remote_copy(
             src_ref=rest_out.at[1, source, :, at], dst_ref=rest_in.at[1, me, :, at],
-            send_sem=q_sent.at[1], recv_sem=q_recv.at[8 + block], device_id=peer,
+            send_sem=sent, recv_sem=q_recv.at[8 + block], device_id=peer,
             device_id_type=MESH,
         )
 
@@ -579,14 +579,14 @@
 
         @pl.when(p == MIDDLE + 10)
         def _():
-            arrived(cw.at[pl.ds(0, 3), pl.ds(0, 128)], cw_sem.at[1])
+            arrived(cw.at[pl.ds(0, 3), pl.ds(0, 128)], cw_sem)
             for k in (1, 3, 2):
                 cs_copy(k).start()
 
         @pl.when(p == MIDDLE + 18)
         def _():
-            arrived(acts.at[pl.ds(0, 3)], act_sem.at[1])
-            arrived(cw.at[pl.ds(0, 3), pl.ds(0, 128)], cs_sem.at[1])
+            arrived(acts.at[pl.ds(0, 3)], act_sem)
+            arrived(cw.at[pl.ds(0, 3), pl.ds(0, 128)], cs_sem)
 
         @pl.when((p >= MIDDLE + 18) & (p < MIDDLE + 22))
         def _():
@@ -651,16 +651,16 @@
 
     with jax.named_scope("s_sent"):
         halo.wait_send()
-        arrived(stat.at[pl.ds(0, 3)], stat_sem.at[0])
-        arrived(acts.at[pl.ds(0, 3)], act_sem.at[0])
-        arrived(cw.at[pl.ds(0, 3), pl.ds(0, 128)], cw_sem.at[0])
-        arrived(cw.at[pl.ds(0, 3), pl.ds(0, 128)], cs_sem.at[0])
-        arrived(sm.at[pl.ds(0, 15)], d_sent.at[0])
-        arrived(sr.at[pl.ds(0, 15)], d_sent.at[1])
-        arrived(bm.at[pl.ds(0, 15), pl.ds(0, 32)], r_sent.at[0])
-        arrived(rest_in.at[0, pl.ds(0, 15)], r_sent.at[1])
-        arrived(bm.at[pl.ds(0, 15), pl.ds(32, 32)], q_sent.at[0])
-        arrived(rest_in.at[1, pl.ds(0, 15)], q_sent.at[1])
+        arrived(stat.at[pl.ds(0, 3)], sent)
+        arrived(acts.at[pl.ds(0, 3)], sent)
+        arrived(cw.at[pl.ds(0, 3), pl.ds(0, 128)], sent)
+        arrived(cw.at[pl.ds(0, 3), pl.ds(0, 128)], sent)
+        arrived(sm.at[pl.ds(0, 15)], sent)
+        arrived(sr.at[pl.ds(0, 15)], sent)
+        arrived(bm.at[pl.ds(0, 15), pl.ds(0, 32)], sent)
+        arrived(rest_in.at[0, pl.ds(0, 15)], sent)
+        arrived(bm.at[pl.ds(0, 15), pl.ds(32, 32)], sent)
+        arrived(rest_in.at[1, pl.ds(0, 15)], sent)
 
         @pl.when(dist < 3)
         def _():
@@ -676,8 +676,8 @@
 def write_out(conv_ref, moe_ref, conv_out, moe_out, sems):
     copies = []
     for source, target in ((moe_ref, moe_out), (conv_ref, conv_out)):
-        for low in range(0, source.shape[0], 128):
-            rows = pl.ds(low, 128)
+        for low in range(0, source.shape[0], OUT_ROWS):
+            rows = pl.ds(low, OUT_ROWS)
             copies.append(
                 pltpu.make_async_copy(source.at[rows], target.at[rows], sems.at[len(copies)])
             )
@@ -746,23 +746,21 @@
             pltpu.VMEM((HALO, channels), bf16),
             pltpu.VMEM((NY, 16, 128), f32),
             pltpu.VMEM((16, 128), f32),
-            dma((10,)),
+            dma((5,)),
             dma((6,)),
             dma((TOTAL,)),
             dma((24,)),
             dma,
             dma,
-            dma((2,)),
+            dma,
             dma((3,)),
             dma((2,)),
-            dma((2,)),
-            dma((2,)),
             dma((12,)),
-            dma((2,)),
-            dma((2,)),
-            dma((2,)),
-            dma((2,)),
-            dma((2,)),
+            dma,
+            dma,
+            dma,
+            dma,
+            dma,
         ],
         compiler_params=pltpu.CompilerParams(
             collective_id=0, has_side_effects=True, vmem_limit_bytes=64_300_000
@@ -789,7 +787,7 @@
         out_shape=tuple(outs),
         in_specs=[vmem, vmem],
         out_specs=(hbm, hbm),
-        scratch_shapes=[dma((sum(out.shape[0] for out in outs) // 128,))],
+        scratch_shapes=[dma((sum(out.shape[0] for out in outs) // OUT_ROWS,))],
         name="write_out",
     )(*(pltpu.with_memory_space_constraint(out, pltpu.VMEM) for out in both))
 

time: 169 us -> 169 us (level)
  no operation moved by 1% of the time
where the time goes in v7:
time: 169 us; the launch traced here: 168 us
  Pallas kernels  168 us (99%)
    pallas_call x1, Pallas kernels, on_device(): pl.pallas_call(kernel, out_shape=(pltpu.VMEM((span // NY, width), bf16),...  166 us

profile of v7, /device:TPU:2, one launch (start us, length us, event | category | flops | bytes accessed | tf_op | source)
XLA Modules:
  0.0 168.3 jit_solution(5113921899891219652)
XLA Ops:
  0.6 166.1 %both.1 = (bf16[256,2048]{1,0:T(8,128)(2,1)S(1)}, bf16[384,2048]{1,0:T(8,128)(2,1)S(1)}) custom-call(bf16[1024,256]{1,0:T(8,128)(2,1)} %value_hbm.1, bf16[1024,256]{1,0:T(8,128)(2,1)} %gate_hbm.1, f32[31,1024]{1,0:T(8,128)} %taps_hbm.1, f32[1,1024]{1,0:T(1,128)} %bitcast.6, f32[1,1024]{1,0:T(1,128)} %bitcast.7, bf16[256,2048]{1,0:T(8,128)(2,1)} %cw_hbm.1, ...), custom_call_target="tpu_custom_call" | custom-call | tf_op jit(solution)/shard_map/both/pallas_call | solution.py:710
  166.7 1.5 write_out.1

commit v8 on v7

--- a/solution.py
+++ b/solution.py
@@ -112,7 +112,7 @@
             pltpu.make_async_copy(
                 ref.at[0, pl.ds(row * PIECE, PIECE), pl.ds(block * 256, 256)],
                 w.at[hs, c, pl.ds(i * PIECE, PIECE)],
-                native.at[i // 8],
+                native.at[i // 16],
             ).start()
 
     for copy in loads:
@@ -154,9 +154,9 @@
         i = expert_at(n)
         mine = (dist == 0) & (i // CHUNKS == c)
 
-        @pl.when(mine & (i % 8 == 0))
-        def _():
-            arrived(w.at[hs, c, pl.ds(0, 8 * PIECE)], native.at[i % CHUNKS // 8])
+        @pl.when(mine & (i % 16 == 0))
+        def _():
+            arrived(w.at[hs, c, pl.ds(0, 16 * PIECE)], native.at[i % CHUNKS // 16])
 
         @pl.when(jnp.logical_not(mine))
         def _():
@@ -255,7 +255,7 @@
         else:
             src, dst = sr.at[block], sx.at[me]
         return pltpu.make_async_remote_copy(
-            src_ref=src, dst_ref=dst, send_sem=sent, recv_sem=d_recv.at[part],
+            src_ref=src, dst_ref=dst, send_sem=sent, recv_sem=d_recv.at[part // 2],
             device_id=(device(z, xx, c), yy), device_id_type=MESH,
         )
 
@@ -387,9 +387,8 @@
         lax.fori_loop(21, START, only_step, 0)
 
     with jax.named_scope("s_wait_rows"):
-        for part in range(2):
-            arrived(rm.at[pl.ds(0, 15), pl.ds(0, 32)], d_recv.at[part])
-        arrived(sx.at[pl.ds(0, 15)], d_recv.at[2])
+        arrived(rm.at[pl.ds(0, 15)], d_recv.at[0])
+        arrived(sx.at[pl.ds(0, 15)], d_recv.at[1])
         rx[...] = sx[...].astype(f32).reshape(128, 2048).astype(bf16)
 
     with jax.named_scope("s_wait_stat"):
@@ -747,13 +746,13 @@
             pltpu.VMEM((NY, 16, 128), f32),
             pltpu.VMEM((16, 128), f32),
             dma((5,)),
-            dma((6,)),
+            dma((3,)),
             dma((TOTAL,)),
             dma((24,)),
             dma,
             dma,
             dma,
-            dma((3,)),
+            dma((2,)),
             dma((2,)),
             dma((12,)),
             dma,

time: 169 us -> 168 us (level)
  no operation moved by 1% of the time
where the time goes in v8:
time: 168 us
  Pallas kernels  168 us (100%)
    pallas_call x1, Pallas kernels, on_device(): pl.pallas_call(kernel, out_shape=(pltpu.VMEM((span // NY, width), bf16),...  166 us

profile of v8, /device:TPU:2, one launch (start us, length us, event | category | flops | bytes accessed | tf_op | source)
XLA Modules:
  0.0 168.2 jit_solution(3329596964036137208)
XLA Ops:
  0.6 166.1 %both.1 = (bf16[256,2048]{1,0:T(8,128)(2,1)S(1)}, bf16[384,2048]{1,0:T(8,128)(2,1)S(1)}) custom-call(bf16[1024,256]{1,0:T(8,128)(2,1)} %value_hbm.1, bf16[1024,256]{1,0:T(8,128)(2,1)} %gate_hbm.1, f32[31,1024]{1,0:T(8,128)} %taps_hbm.1, f32[1,1024]{1,0:T(1,128)} %bitcast.6, f32[1,1024]{1,0:T(1,128)} %bitcast.7, bf16[256,2048]{1,0:T(8,128)(2,1)} %cw_hbm.1, ...), custom_call_target="tpu_custom_call" | custom-call | tf_op jit(solution)/shard_map/both/pallas_call | solution.py:709
  166.7 1.5 write_out.1
